TPU v7x, 32 devices: a whole 2x2x4 slice. The times are simulated.
32 devices in a mesh: fs: 4 (over z), rep: 4 (over y, x), tp: 2 (over core).
Axes of the slice: x: 2, y: 2, z: 4, core: 2. Of those that a mesh axis runs over, the one named last changes fastest.
Arguments:
- saved_input: bfloat16 [32768, 2048], P(('fs', 'rep')), may hold values from -8 to 8
- query_cotangent: bfloat16 [32768, 1024], P(('fs', 'rep'), 'tp'), may hold values from -0.03125 to 0.03125
- saved_heads: bfloat16 [32768, 1024], P(('fs', 'rep'), 'tp'), may hold values from -6 to 6
- block_cotangent: bfloat16 [32768, 2048], P(('fs', 'rep')), may hold values from -0.046875 to 0.046875
- query_weight: float32 [2048, 1024], P(('fs', 'rep'), 'tp'), may hold values from -6 to 6
- output_weight: float32 [1024, 2048], P('tp', ('fs', 'rep')), may hold values from -6 to 6
- query_factor: bfloat16 [2048, 256], P(('fs', 'rep')), may hold values from -0.125 to 0.125
- output_factor: bfloat16 [2048, 256], P(('fs', 'rep')), may hold values from -0.125 to 0.125
- query_first: float32 [256, 1024], P(None, 'tp'), may hold values from -6 to 6
- query_second: float32 [256, 1024], P(None, 'tp'), may hold values from 0.5 to 2
- output_first: float32 [1024, 256], P('tp'), may hold values from -6 to 6
- output_second: float32 [1024, 256], P('tp'), may hold values from 0.5 to 2
Outputs:
- new_query_weight: float32 [2048, 1024], P(('fs', 'rep'), 'tp')
- new_output_weight: float32 [1024, 2048], P('tp', ('fs', 'rep'))
- new_query_first: float32 [256, 1024], P(None, 'tp')
- new_query_second: float32 [256, 1024], P(None, 'tp')
- new_output_first: float32 [1024, 256], P('tp')
- new_output_second: float32 [1024, 256], P('tp')
- query_step: float32 [2048, 1024], P(('fs', 'rep'), 'tp')
- output_step: float32 [1024, 2048], P('tp', ('fs', 'rep'))
- query_copy: bfloat16 [2048, 1024], P(None, 'tp')
- output_copy: bfloat16 [1024, 2048], P('tp')
All inputs are finite; a program needn't handle non-finite values.
Results may differ from a plain program's by a relative error of at most 0.0013.
Values may be sent and summed in bfloat16 or wider, within the bound.
A program may use at most 128 MiB of HBM per device.

v0:
```python
import functools

import jax
import jax.numpy as jnp
from jax import lax
from jax.experimental import pallas as pl
from jax.experimental.pallas import tpu as pltpu
from jax.sharding import PartitionSpec as P

MESH = pl.DeviceIdType.MESH
BF = jnp.bfloat16
F32 = jnp.float32


def split_parts(wide):
    upper = wide.astype(BF)
    lower = (wide - upper.astype(F32)).astype(BF)
    return (upper, lower)


REACH = 6.0
MANTISSA = 128
SPAN = 120
LEVELS = 2 * SPAN * MANTISSA


def encode(weight):
    scaled = jnp.sqrt(jnp.minimum(jnp.abs(weight), REACH) / REACH) * LEVELS
    level = jnp.minimum(jnp.floor(scaled + 0.5), LEVELS - 1)
    power = jnp.floor(level / MANTISSA)
    fraction = (level - power * MANTISSA) / MANTISSA
    size = jnp.exp2(power - SPAN) * (1.0 + fraction)
    return jnp.where(weight < 0, -size, size).astype(BF)


def decode(code):
    wide = code.astype(F32)
    size = jnp.abs(wide)
    power = jnp.floor(jnp.log2(size) + 0.002)
    fraction = jnp.floor((size * jnp.exp2(-power) - 1.0) * MANTISSA + 0.5)
    level = ((power + SPAN) * MANTISSA + fraction) * (1.0 / LEVELS)
    value = REACH * level * level
    return jnp.where(wide < 0, -value, value)


def remote(src, dst, send, recv, where):
    copy = pltpu.make_async_remote_copy(
        src_ref=src, dst_ref=dst, send_sem=send, recv_sem=recv, device_id=where, device_id_type=MESH
    )
    return copy


def place(nf, nr):
    f, r, t = lax.axis_index("fs"), lax.axis_index("rep"), lax.axis_index("tp")
    near = r + 1 - 2 * lax.rem(r, 2)
    side = lax.rem(r + 2, 4)
    far = 3 - r
    return f, r, t, near, side, far


def greet(nf, f, near, side, far, t):
    barrier = pltpu.get_barrier_semaphore()
    for df in range(1, nf):
        pl.semaphore_signal(barrier, inc=1, device_id={"fs": lax.rem(f + df, nf)}, device_id_type=MESH)
    for peer in (near, side, far):
        pl.semaphore_signal(barrier, inc=1, device_id={"rep": peer}, device_id_type=MESH)
    pl.semaphore_signal(barrier, inc=1, device_id={"tp": 1 - t}, device_id_type=MESH)
    pl.semaphore_wait(barrier, nf - 1 + 4)


def gather(nf, nr, f, r, near, side, far, parts, first, second, sems, passed=None, started=None):
    fs_s, fs_r, n_s, n_r, s_s, s_r, d_s, d_r = sems
    width = len(parts(0))
    half = len(first(0))
    me = f * nr + r
    sent = []

    def send(refs, send_sem, recv_sem, row, where):
        got = []
        for k, ref in enumerate(refs):
            copy = remote(ref, ref, send_sem.at[row, k], recv_sem.at[row, k], where)
            copy.start()
            got.append(copy)
        sent.extend(got)

    def arrive(refs, send_sem, recv_sem, row, where):
        for k, ref in enumerate(refs):
            remote(ref, ref, send_sem.at[row, k], recv_sem.at[row, k], where).wait_recv()

    send(parts(me), n_s, n_r, 0, {"rep": near})
    send(parts(me), s_s, s_r, 0, {"rep": side})
    for df in range(1, nf):
        send(parts(me), fs_s, fs_r, df, {"fs": lax.rem(f + df, nf)})
    if started:
        started()
    for df in range(nf):
        from_f = lax.rem(f + nf - df, nf)
        if df > 0:
            slot = from_f * nr + r
            arrive(parts(slot), fs_s, fs_r, df, {"fs": from_f})
            send(parts(slot), n_s, n_r, df, {"rep": near})
            send(parts(slot), s_s, s_r, df, {"rep": side})
            if passed:
                passed(slot)
        if df > 0:
            relay(nf, nr, f, near, side, df - 1, parts, first, second, arrive, send, sems, passed)
    relay(nf, nr, f, near, side, nf - 1, parts, first, second, arrive, send, sems, passed)
    for df in range(nf):
        slot = lax.rem(f + nf - df, nf) * nr + far
        arrive(first(slot), d_s.at[0], d_r.at[0], df, {"rep": side})
        arrive(second(slot), d_s.at[1], d_r.at[1], df, {"rep": near})
        if passed:
            passed(slot)
    for copy in sent:
        copy.wait_send()


def relay(nf, nr, f, near, side, df, parts, first, second, arrive, send, sems, passed):
    fs_s, fs_r, n_s, n_r, s_s, s_r, d_s, d_r = sems
    from_f = lax.rem(f + nf - df, nf)
    one = from_f * nr + near
    arrive(parts(one), n_s, n_r, df, {"rep": near})
    send(first(one), d_s.at[0], d_r.at[0], df, {"rep": side})
    two = from_f * nr + side
    arrive(parts(two), s_s, s_r, df, {"rep": side})
    send(second(two), d_s.at[1], d_r.at[1], df, {"rep": near})
    if passed:
        passed(one)
        passed(two)


def gather_sems(nf, width, half):
    dma = pltpu.SemaphoreType.DMA
    return [dma((nf, width))] * 6 + [dma((2, nf, half))] * 2


def factor_kernel(nf, nr, fq_ref, fo_ref, wq_ref, wo_ref, out_ref, colq_ref, colo_ref, *sems):
    f, r, t, near, side, far = place(nf, nr)
    local, p_s, p_r, w_s, w_r = sems[8:]
    me = f * nr + r
    rows = fq_ref.shape[0]
    copies = [
        pltpu.make_async_copy(fq_ref, out_ref.at[0, me], local.at[0]),
        pltpu.make_async_copy(fo_ref, out_ref.at[1, me], local.at[1]),
        pltpu.make_async_copy(wq_ref, colq_ref.at[f], local.at[2]),
        pltpu.make_async_copy(wo_ref, colo_ref.at[f], local.at[3]),
    ]
    for copy in copies:
        copy.start()
    greet(nf, f, near, side, far, t)
    for copy in copies:
        copy.wait()
    relayed = []

    def columns():
        for df in range(1, nf):
            to = lax.rem(f + df, nf)
            for k, (own, ref) in enumerate(((wq_ref, colq_ref), (wo_ref, colo_ref))):
                remote(own, ref.at[f], w_s.at[k, df], w_r.at[k, df], {"fs": to}).start()

    def passed(slot):
        copy = remote(
            out_ref.at[t, slot], out_ref.at[t, slot], p_s.at[len(relayed)], p_r.at[len(relayed)], {"tp": 1 - t}
        )
        copy.start()
        relayed.append(slot)

    gather(
        nf, nr, f, r, near, side, far,
        lambda s: [out_ref.at[t, s]],
        lambda s: [out_ref.at[t, s, pl.ds(0, rows // 2)]],
        lambda s: [out_ref.at[t, s, pl.ds(rows // 2, rows // 2)]],
        sems[:8],
        passed,
        columns,
    )
    for df in range(1, nf):
        from_f = lax.rem(f + nf - df, nf)
        for k, ref in enumerate((colq_ref, colo_ref)):
            copy = remote(ref.at[from_f], ref.at[from_f], w_s.at[k, df], w_r.at[k, df], {"fs": from_f})
            copy.wait_recv()
            copy.wait_send()
    for k, slot in enumerate(relayed):
        copy = remote(out_ref.at[t, slot], out_ref.at[t, slot], p_s.at[k], p_r.at[k], {"tp": 1 - t})
        copy.wait_send()
        remote(out_ref.at[1 - t, slot], out_ref.at[1 - t, slot], p_s.at[k], p_r.at[k], {"tp": 1 - t}).wait_recv()


def update_kernel(
    nf, nr, wide,
    part_ref, factor_ref, colq_ref, colo_ref, wq_ref, wo_ref, fq_ref, sq_ref, fo_ref, so_ref,
    nwq_ref, nwo_ref, nfq_ref, nsq_ref, nfo_ref, nso_ref, stq_ref, sto_ref, cq_ref, co_ref,
    outgoing, landed, partial, exchanged, whole, dirs, flat, gotq, goto, square, *sems,
):
    f, r, t, near, side, far = place(nf, nr)
    a_s, a_r, b_s, b_r, c_s, c_r, e_s, e_r, x_s, x_r, w_s, w_r = sems
    n = nf * nr
    me = f * nr + r
    depth = factor_ref.shape[2]
    rank = dirs.shape[2]
    for k in range(nr):
        outgoing[k] = part_ref[k].astype(BF)
    greet(nf, f, near, side, far, t)
    sent = []
    peers = (near, side, far)
    for k, peer in enumerate(peers):
        copy = remote(outgoing.at[peer], landed.at[k], a_s.at[k], a_r.at[k], {"rep": peer})
        copy.start()
        sent.append(copy)

    def spread_column(fi):
        for k, peer in enumerate((near, side)):
            for half, (own, ref) in enumerate(((colq_ref, gotq), (colo_ref, goto))):
                copy = remote(own.at[fi], ref.at[k, fi], w_s.at[k, half, fi], w_r.at[k, half, fi], {"rep": peer})
                copy.start()
                sent.append(copy)

    def relay_column(fi):
        for k, peer in enumerate((near, side)):
            for half, (own, ref) in enumerate(((colq_ref, gotq), (colo_ref, goto))):
                remote(own.at[fi], ref.at[k, fi], w_s.at[k, half, fi], w_r.at[k, half, fi], {"rep": peer}).wait_recv()
        for k, ref, peer in ((0, gotq, side), (1, goto, near)):
            copy = remote(ref.at[k, fi], ref.at[2, fi], w_s.at[2, k, fi], w_r.at[2, k, fi], {"rep": peer})
            copy.start()
            sent.append(copy)

    for fi in range(nf // 2):
        spread_column(fi)
    for k, peer in enumerate(peers):
        remote(outgoing.at[peer], landed.at[k], a_s.at[k], a_r.at[k], {"rep": peer}).wait_recv()
    total = part_ref[r] + landed[0].astype(F32) + landed[1].astype(F32) + landed[2].astype(F32)
    partial[...] = total.astype(BF)
    for df in range(1, nf):
        to = lax.rem(f + df, nf)
        copy = remote(partial.at[to], exchanged.at[df], b_s.at[df], b_r.at[df], {"fs": to})
        copy.start()
        sent.append(copy)
    mine = part_ref[r, f] + landed[0, f].astype(F32) + landed[1, f].astype(F32) + landed[2, f].astype(F32)
    for df in range(1, nf):
        remote(partial.at[f], exchanged.at[df], b_s.at[df], b_r.at[df], {"fs": f}).wait_recv()
        mine = mine + exchanged[df].astype(F32)
    whole[r, f] = mine.astype(BF)
    for df in range(nf):
        from_f = lax.rem(f + nf - df, nf)
        if df == 0:
            for step in range(1, nf):
                copy = remote(
                    whole.at[r, f], whole.at[r, f], c_s.at[step], c_r.at[step], {"fs": lax.rem(f + step, nf)}
                )
                copy.start()
                sent.append(copy)
        else:
            ref = whole.at[r, from_f]
            remote(ref, ref, c_s.at[df], c_r.at[df], {"fs": from_f}).wait_recv()
        for k, peer in enumerate(peers):
            ref = whole.at[r, from_f]
            copy = remote(ref, ref, e_s.at[k, df], e_r.at[k, df], {"rep": peer})
            copy.start()
            sent.append(copy)
    for fi in range(nf // 2, nf):
        spread_column(fi)
    for fi in range(nf // 2):
        relay_column(fi)
    for df in range(nf):
        from_f = lax.rem(f + nf - df, nf)
        for k, peer in enumerate(peers):
            ref = whole.at[peer, from_f]
            remote(ref, ref, e_s.at[k, df], e_r.at[k, df], {"rep": peer}).wait_recv()
    rows = nr // 2
    cols = part_ref.shape[3]
    for which, first, second, new_first, new_second in (
        (0, fq_ref, sq_ref, nfq_ref, nsq_ref),
        (1, fo_ref, so_ref, nfo_ref, nso_ref),
    ):
        proj = whole[which * rows : (which + 1) * rows].astype(F32).reshape(rank, cols)
        if which:
            proj = proj.T
        moved = 0.9 * first[...] + 0.1 * proj
        spread = 0.95 * second[...] + 0.05 * proj * proj
        new_first[...] = moved
        new_second[...] = spread
        way = moved / (jnp.sqrt(spread) + 1e-08)
        if which:
            flat[0], flat[1] = split_parts(way)
            way = way.T
        upper, lower = split_parts(way)
        dirs[which, 0] = upper
        dirs[which, 1] = lower

    def turned(slot):
        across = (((1,), (1,)), ((), ()))
        block = factor_ref[1, slot]
        return lax.dot_general(flat[0], block, across, preferred_element_type=F32) + lax.dot_general(
            flat[1], block, across, preferred_element_type=F32
        )

    def raw_of(which, slot):
        block = factor_ref[which, slot]
        return jnp.dot(block, dirs[which, 0], preferred_element_type=F32) + jnp.dot(
            block, dirs[which, 1], preferred_element_type=F32
        )

    for which in range(2):
        def add(slot, carry):
            raw = raw_of(which, slot)
            return carry + jnp.sum((raw * raw).reshape(depth // 8, 8, cols), axis=0)

        tally = lax.fori_loop(0, n, add, jnp.zeros((8, cols), F32))
        square[0, which] = tally
    copy = remote(square.at[0], square.at[1], x_s, x_r, {"tp": 1 - t})
    copy.start()
    for fi in range(nf // 2, nf):
        relay_column(fi)
    copy.wait()
    entries = wide * cols * 2
    sums = [
        jnp.sum(square[0, which] + square[1, which]) / entries + 0.01 for which in range(2)
    ]
    for raw, mean, weight, new_weight, step_ref, which in (
        (raw_of(0, me), sums[0], wq_ref, nwq_ref, stq_ref, 0),
        (turned(me), sums[1], wo_ref, nwo_ref, sto_ref, 1),
    ):
        step = raw / jnp.sqrt(jnp.full(raw.shape, mean, F32))
        new = weight[...] - 0.1 * step
        step_ref[...] = step
        new_weight[...] = new

    rate = [0.1 / jnp.sqrt(jnp.full((1, 1), mean, F32)) for mean in sums]

    def finish(pick_q, pick_o, row):
        def one(fi, carry):
            slot = fi * nr + row
            cq_ref[slot] = (decode(pick_q(fi)) - rate[0] * raw_of(0, slot)).astype(BF)
            new = (decode(pick_o(fi)) - rate[1] * turned(slot)).astype(BF)
            if depth % 128 == 0:
                co_ref[:, pl.ds(pl.multiple_of(slot * depth, 128), depth)] = new
            else:
                co_ref[slot] = new
            return carry

        lax.fori_loop(0, nf, one, 0)

    finish(lambda fi: colq_ref[fi], lambda fi: colo_ref[fi], r)
    finish(lambda fi: gotq[0, fi], lambda fi: goto[0, fi], near)
    finish(lambda fi: gotq[1, fi], lambda fi: goto[1, fi], side)
    for fi in range(nf):
        for k, ref, peer in ((0, gotq, side), (1, goto, near)):
            remote(ref.at[k, fi], ref.at[2, fi], w_s.at[2, k, fi], w_r.at[2, k, fi], {"rep": peer}).wait_recv()
    finish(lambda fi: gotq[2, fi], lambda fi: goto[2, fi], far)
    for copy in sent:
        copy.wait_send()


def store_kernel(count, *refs):
    ins, outs, sems = refs[:count], refs[count : 2 * count], refs[2 * count]
    copies = [pltpu.make_async_copy(ins[k], outs[k], sems.at[k]) for k in range(count)]
    for copy in copies:
        copy.start()
    for copy in copies:
        copy.wait()


def store(arrays):
    count = len(arrays)
    return pl.pallas_call(
        functools.partial(store_kernel, count),
        out_shape=[jax.ShapeDtypeStruct(a.shape, a.dtype) for a in arrays],
        in_specs=[pl.BlockSpec(memory_space=pltpu.VMEM)] * count,
        out_specs=[pl.BlockSpec(memory_space=pl.ANY)] * count,
        scratch_shapes=[pltpu.SemaphoreType.DMA((count,))],
        compiler_params=pltpu.CompilerParams(vmem_limit_bytes=16 * 1024 * 1024),
    )(*arrays)


def body(
    nf, nr,
    saved_input, query_cotangent, saved_heads, block_cotangent, query_weight, output_weight,
    query_factor, output_factor, query_first, query_second, output_first, output_second,
):
    contract = (((0,), (0,)), ((), ()))
    n = nf * nr
    depth, rank = query_factor.shape
    cols = query_weight.shape[1]
    dma = pltpu.SemaphoreType.DMA
    vmem = pl.BlockSpec(memory_space=pltpu.VMEM)
    factors, column_q, column_o = pl.pallas_call(
        functools.partial(factor_kernel, nf, nr),
        out_shape=[
            jax.ShapeDtypeStruct((2, n, depth, rank), BF),
            jax.ShapeDtypeStruct((nf, depth, cols), BF),
            jax.ShapeDtypeStruct((nf, cols, depth), BF),
        ],
        in_specs=[vmem] * 4,
        out_specs=[vmem] * 3,
        scratch_shapes=gather_sems(nf, 1, 1) + [dma((4,)), dma((n,)), dma((n,)), dma((2, nf)), dma((2, nf))],
        compiler_params=pltpu.CompilerParams(
            collective_id=0, has_side_effects=True, vmem_limit_bytes=12 * 1024 * 1024
        ),
    )(query_factor, output_factor, encode(query_weight), encode(output_weight))
    whole_q = factors[0].reshape(n * depth, rank)
    whole_o = factors[1].reshape(n * depth, rank)
    input_low = jnp.dot(saved_input, whole_q, preferred_element_type=F32)
    cotan_low = jnp.dot(block_cotangent, whole_o, preferred_element_type=F32)
    input_upper, input_lower = split_parts(input_low)
    cotan_upper, cotan_lower = split_parts(cotan_low)
    part_query = lax.dot_general(
        input_upper, query_cotangent, contract, preferred_element_type=F32
    ) + lax.dot_general(input_lower, query_cotangent, contract, preferred_element_type=F32)
    part_output = lax.dot_general(
        cotan_upper, saved_heads, contract, preferred_element_type=F32
    ) + lax.dot_general(cotan_lower, saved_heads, contract, preferred_element_type=F32)
    rows = 2 * rank // n
    part = jnp.concatenate([part_query, part_output], axis=0).reshape(nr, nf, rows, cols)
    aligned = depth % 128 == 0
    shape = jax.ShapeDtypeStruct
    outs = pl.pallas_call(
        functools.partial(update_kernel, nf, nr, n * depth),
        out_shape=[
            shape((depth, cols), F32), shape((cols, depth), F32),
            shape((rank, cols), F32), shape((rank, cols), F32),
            shape((cols, rank), F32), shape((cols, rank), F32),
            shape((depth, cols), F32), shape((cols, depth), F32),
            shape((n, depth, cols), BF),
            shape((cols, n * depth) if aligned else (n, cols, depth), BF),
        ],
        in_specs=[vmem] * 10,
        out_specs=[vmem] * 10,
        scratch_shapes=[
            pltpu.VMEM((nr, nf, rows, cols), BF),
            pltpu.VMEM((3, nf, rows, cols), BF),
            pltpu.VMEM((nf, rows, cols), BF),
            pltpu.VMEM((nf, rows, cols), BF),
            pltpu.VMEM((nr, nf, rows, cols), BF),
            pltpu.VMEM((2, 2, rank, cols), BF),
            pltpu.VMEM((2, cols, rank), BF),
            pltpu.VMEM((3, nf, depth, cols), BF),
            pltpu.VMEM((3, nf, cols, depth), BF),
            pltpu.VMEM((2, 2, 8, cols), F32),
        ]
        + [dma((3,)), dma((3,)), dma((nf,)), dma((nf,)), dma((nf,)), dma((nf,)), dma((3, nf)), dma((3, nf)), dma, dma]
        + [dma((3, 2, nf))] * 2,
        compiler_params=pltpu.CompilerParams(
            collective_id=1, has_side_effects=True, vmem_limit_bytes=40 * 1024 * 1024
        ),
    )(part, factors, column_q, column_o, query_weight, output_weight, query_first, query_second, output_first, output_second)
    *rest, query_copy, output_copy = store(outs)
    query_copy = query_copy.reshape(n * depth, cols)
    if not aligned:
        output_copy = output_copy.transpose(1, 0, 2).reshape(cols, n * depth)
    return (*rest, query_copy, output_copy)


def solution(mesh):
    nf, nr = mesh.shape["fs"], mesh.shape["rep"]
    in_specs = (
        P(("fs", "rep"), None), P(("fs", "rep"), "tp"), P(("fs", "rep"), "tp"), P(("fs", "rep"), None),
        P(("fs", "rep"), "tp"), P("tp", ("fs", "rep")), P(("fs", "rep"), None), P(("fs", "rep"), None),
        P(None, "tp"), P(None, "tp"), P("tp", None), P("tp", None),
    )
    out_specs = (
        P(("fs", "rep"), "tp"), P("tp", ("fs", "rep")), P(None, "tp"), P(None, "tp"), P("tp", None), P("tp", None),
        P(("fs", "rep"), "tp"), P("tp", ("fs", "rep")), P(None, "tp"), P("tp", None),
    )
    return jax.shard_map(
        functools.partial(body, nf, nr), mesh=mesh, in_specs=in_specs, out_specs=out_specs, check_vma=False
    )
```

profile of v0, /device:TPU:0, one launch (start us, length us, event | category | flops | bytes accessed | tf_op | source)
XLA Modules:
  0.0 108.2 jit_solution(17934780077175880971)
XLA Ops:
  0.6 0.0 copy-start
  0.7 1.4 %fusion.6.wq_ref = bf16[128,512]{1,0:T(8,128)(2,1)S(1)} fusion(f32[128,512]{1,0:T(8,128)} %wq_ref.1), kind=kLoop, calls=%fused_computation.15 | loop fusion | flops 1310720 | bytes 393216 | tf_op jit(solution)/shard_map/convert_element_type | solution.py:33
  2.0 1.2 %fusion.7.wo_ref = bf16[512,128]{1,0:T(8,128)(2,1)S(1)} fusion(f32[512,128]{1,0:T(8,128)} %wo_ref.1), kind=kLoop, calls=%fused_computation.16 | loop fusion | flops 1310720 | bytes 393216 | tf_op jit(solution)/shard_map/convert_element_type | solution.py:33
  3.2 0.0 copy-start.7
  3.2 0.8 copy-done.7
  4.1 0.0 copy-start.8
  4.1 0.8 copy-done.8
  4.9 31.9 %shard_map.195 = (bf16[2,16,128,256]{3,2,1,0:T(8,128)(2,1)S(1)}, bf16[4,128,512]{2,1,0:T(8,128)(2,1)S(1)}, bf16[4,512,128]{2,1,0:T(8,128)(2,1)S(1)}) custom-call(bf16[128,256]{1,0:T(8,128)(2,1)S(1)} %copy-done.7, bf16[128,256]{1,0:T(8,128)(2,1)S(1)} %copy-done.8, bf16[128,512]{1,0:T(8,128)(2,1)S(1)} %fusion.6.wq_ref, bf16[512,128]{1,0:T(8,128)(2,1)S(1)} %fusion.7.wo_ref), custom_call_target="tpu_custom_call" | custom-call | tf_op jit(solution)/shard_map/pallas_call | solution.py:386
  36.8 0.0 slice-start
  36.8 0.2 fusion.8
  37.0 0.0 slice-start.1
  37.0 5.9 %convolution_bitcast_fusion = f32[2048,256]{0,1:T(8,128)S(1)} fusion(bf16[2048,256]{1,0:T(8,128)(2,1)S(1)} %bitcast.18, bf16[2048,2048]{1,0:T(8,128)(2,1)} %param.15), kind=kOutput, calls=%fused_computation | convolution fusion | flops 2147483648 | bytes 11534336 | tf_op jit(solution)/shard_map/dot_general | solution.py:403
  43.0 0.0 copy-done
  43.0 0.7 fusion.1
  43.7 0.7 convolution_add_fusion
  44.4 0.0 slice-done
  44.4 0.0 slice-done.1
  44.4 0.0 copy-start.9
  44.4 2.4 %convolution_bitcast_fusion.1 = f32[2048,256]{0,1:T(8,128)S(1)} fusion(bf16[2048,256]{1,0:T(8,128)(2,1)S(1)} %bitcast.17, bf16[2048,2048]{1,0:T(8,128)(2,1)S(1)} %bitcast.20), kind=kOutput, calls=%fused_computation.1 | convolution fusion | flops 2147483648 | bytes 11534336 | tf_op jit(solution)/shard_map/dot_general | solution.py:402
  46.8 0.0 copy-done.9
  46.8 0.7 fusion.4
  47.6 0.0 copy-start.6
  47.6 0.7 convolution_add_fusion.1
  48.3 0.0 copy-start.1
  48.3 0.0 copy-start.2
  48.3 0.0 copy-start.3
  48.3 0.0 copy-start.4
  48.3 0.0 copy-start.5
  48.3 0.1 pad_maximum_fusion
  48.4 0.2 copy-done.6
  48.6 0.7 copy-done.1
  49.3 0.1 copy-done.2
  49.3 0.2 copy-done.3
  49.5 0.2 copy-done.4
  49.7 0.2 copy-done.5
  49.8 55.2 %shard_map.196 = (f32[128,512]{1,0:T(8,128)S(1)}, f32[512,128]{1,0:T(8,128)S(1)}, f32[256,512]{1,0:T(8,128)S(1)}, f32[256,512]{1,0:T(8,128)S(1)}, f32[512,256]{1...) custom-call(f32[4,4,32,512]{3,2,1,0:T(8,128)S(1)} %bitcast.16, ...), custom_call_target="tpu_custom_call" | custom-call | tf_op jit(solution)/shard_map/pallas_call | solution.py:416
  105.1 3.1 %shard_map.197 = (f32[128,512]{1,0:T(8,128)}, f32[512,128]{1,0:T(8,128)}, f32[256,512]{1,0:T(8,128)}, f32[256,512]{1,0:T(8,128)}, f32[512,256]{1,0:T(8,128)}, /*...) custom-call(f32[128,512]{1,0:T(8,128)S(1)} %get-tuple-element.36.ref, ...), custom_call_target="tpu_custom_call" | custom-call | tf_op jit(solution)/shard_map/pallas_call | solution.py:365
  (1 shorter events, 0.0 us)
Async XLA Ops:
  0.6 42.3 %copy-start = (bf16[2048,512]{1,0:T(8,128)(2,1)S(1)}, bf16[2048,512]{1,0:T(8,128)(2,1)}, u32[]{:S(2)}) copy-start(bf16[2048,512]{1,0:T(8,128)(2,1)} %param.14) | copy-start | bytes 6291460
  3.2 0.8 copy-start.7
  4.1 0.8 copy-start.8
  36.8 7.6 %slice-start = ((s8[8388608]{0:T(1024)(128)(4,1)}), s8[4194304]{0:T(1024)(128)(4,1)S(1)}, s32[]{:S(2)}) async-start(s8[8388608]{0:T(1024)(128)(4,1)} %bitcast.19), calls=%async_computation | async-start | bytes 8388608
  37.0 7.4 %slice-start.1 = ((s8[8388608]{0:T(1024)(128)(4,1)}), s8[4194304]{0:T(1024)(128)(4,1)S(1)}, s32[]{:S(2)}) async-start(s8[8388608]{0:T(1024)(128)(4,1)} %bitcast.19), calls=%async_computation.1 | async-start | bytes 8388608
  44.4 2.4 %copy-start.9 = (bf16[2048,512]{1,0:T(8,128)(2,1)S(1)}, bf16[2048,512]{1,0:T(8,128)(2,1)}, u32[]{:S(2)}) copy-start(bf16[2048,512]{1,0:T(8,128)(2,1)} %param.13) | copy-start | bytes 6291460
  47.6 1.0 copy-start.6
  48.3 1.0 copy-start.1
  48.3 1.1 copy-start.2
  48.3 1.2 %copy-start.3 = (f32[256,512]{1,0:T(8,128)S(1)}, f32[256,512]{1,0:T(8,128)}, u32[]{:S(2)}) copy-start(f32[256,512]{1,0:T(8,128)} %fq_ref.3) | copy-start | bytes 1572868
  48.3 1.4 %copy-start.4 = (f32[256,512]{1,0:T(8,128)S(1)}, f32[256,512]{1,0:T(8,128)}, u32[]{:S(2)}) copy-start(f32[256,512]{1,0:T(8,128)} %sq_ref.1) | copy-start | bytes 1572868
  48.3 1.5 %copy-start.5 = (f32[512,256]{1,0:T(8,128)S(1)}, f32[512,256]{1,0:T(8,128)}, u32[]{:S(2)}) copy-start(f32[512,256]{1,0:T(8,128)} %fo_ref.3) | copy-start | bytes 1572868
where the time goes:
time: 109 us; the launch traced here: 108 us
  Pallas kernels  90.3 us (83%)
  matrix products  11.1 us (10%)
  local copies, waits for them, and re-layouts  3.36 us (3%)
  other arithmetic  2.63 us (2%)
    pallas_call x1, Pallas kernels, body(): pl.pallas_call(functools.partial(update_kernel, nf, nr, n * depth), out_s...  55.2 us
    pallas_call x1, Pallas kernels, body(): pl.pallas_call(functools.partial(factor_kernel, nf, nr), out_shape=[jax.S...  31.9 us
    dot_general x1, matrix products, body(): cotan_low = jnp.dot(block_cotangent, whole_o, preferred_element_type=F32)  5.92 us
    unnamed x24, local copies, waits for them, and re-layouts  3.15 us
    pallas_call x1, Pallas kernels, store(): pl.pallas_call(functools.partial(store_kernel, count), out_shape=[jax.Sha...  3.14 us
    convert_element_type x2, other arithmetic, encode(): return jnp.where(weight < 0, -size, size).astype(BF)  2.56 us
    dot_general x1, matrix products, body(): input_low = jnp.dot(saved_input, whole_q, preferred_element_type=F32)  2.39 us

commit v1 on v0

v1 whole, which is shorter than its diff:
```python
import functools

import jax
import jax.numpy as jnp
from jax import lax
from jax.experimental import pallas as pl
from jax.experimental.pallas import tpu as pltpu
from jax.sharding import PartitionSpec as P

MESH = pl.DeviceIdType.MESH
BF = jnp.bfloat16
F32 = jnp.float32

REACH = 6.0
SPAN = 120.0
PER_LOG = 1.0 / (2.0 * SPAN * 0.6931471805599453)


def split_parts(wide):
    upper = wide.astype(BF)
    lower = (wide - upper.astype(F32)).astype(BF)
    return (upper, lower)


def encode(weight):
    level = jnp.sqrt(jnp.minimum(jnp.abs(weight), REACH) * (1.0 / REACH))
    size = jnp.exp2(level * (2.0 * SPAN) - SPAN)
    return jnp.where(weight < 0, -size, size).astype(BF)


def decode(code):
    wide = code.astype(F32)
    level = jnp.log(jnp.abs(wide)) * PER_LOG + 0.5
    value = (REACH * level) * level
    return jnp.where(wide < 0, -value, value)


def remote(src, dst, send, recv, where):
    return pltpu.make_async_remote_copy(
        src_ref=src, dst_ref=dst, send_sem=send, recv_sem=recv, device_id=where, device_id_type=MESH
    )


def nth_plane(f, nf, j):
    if j == 0:
        return f, 1
    upper = (2 * f) // nf
    near_end = f + upper * (nf - 1 - 2 * f)
    over = jnp.minimum(1, j // (2 * near_end + 1))
    inner_sign = 1 if j % 2 else -1
    distance = over * (j - near_end) + (1 - over) * ((j + 1) // 2)
    sign = (1 - 2 * upper) * (over + (1 - over) * inner_sign)
    return f + sign * distance, sign


def update_kernel(
    nf, nr, wide, cut,
    x_hbm, bc_hbm, qc_hbm, sh_hbm, wq_hbm, wo_hbm, fq_hbm, fo_hbm, mq_hbm, vq_hbm, mo_hbm, vo_hbm,
    nwq_ref, nwo_ref, nfq_ref, nsq_ref, nfo_ref, nso_ref, stq_ref, sto_ref, cq_ref, co_ref,
    xs, cots, fb, wq_ref, wo_ref, cwq, cwo, low, lows,
    outgoing, landed, own, partial, exchanged, whole, dirs, flat, square,
    loc, fz_s, fz_r, fn_s, fn_r, fd_s, fd_r, fp_s, fp_r, wn_s, wn_r, wd_s, wd_r, wz_s, wz_r,
    a_s, a_r, b_s, b_r, c_s, c_r, e_s, e_r, x_s, x_r,
):
    f, r, t = lax.axis_index("fs"), lax.axis_index("rep"), lax.axis_index("tp")
    near = r + 1 - 2 * lax.rem(r, 2)
    side = lax.rem(r + 2, 4)
    far = 3 - r
    n = nf * nr
    me = f * nr + r
    depth, rank = fq_hbm.shape
    cols = wq_hbm.shape[1]
    tokens = x_hbm.shape[0]
    lane = nr * depth
    quarter = 2 * rank // nr
    rows = quarter // nf
    peers = (near, side, far)
    aligned = depth % 128 == 0

    local = []

    def fetch(src, dst):
        copy = pltpu.make_async_copy(src, dst, loc.at[len(local)])
        copy.start()
        local.append(copy)
        return copy

    small = [fetch(fq_hbm, fb.at[0, me]), fetch(fo_hbm, fb.at[1, me])]
    weights = [fetch(wq_hbm, wq_ref), fetch(wo_hbm, wo_ref)]
    barrier = pltpu.get_barrier_semaphore()
    for df in range(1, nf):
        pl.semaphore_signal(barrier, inc=1, device_id={"fs": lax.rem(f + df, nf)}, device_id_type=MESH)
    for peer in peers:
        pl.semaphore_signal(barrier, inc=1, device_id={"rep": peer}, device_id_type=MESH)
    pl.semaphore_signal(barrier, inc=1, device_id={"tp": 1 - t}, device_id_type=MESH)
    big = [fetch(x_hbm, xs.at[0]), fetch(bc_hbm, xs.at[1]), fetch(qc_hbm, cots.at[0]), fetch(sh_hbm, cots.at[1])]
    moments = [fetch(a, b) for a, b in ((mq_hbm, nfq_ref), (vq_hbm, nsq_ref), (mo_hbm, nfo_ref), (vo_hbm, nso_ref))]
    for copy in small:
        copy.wait()
    pl.semaphore_wait(barrier, nf - 1 + 4)

    sent = []

    def send(src, dst, send_sem, recv_sem, where, when=None):
        def make():
            return remote(src, dst, send_sem, recv_sem, where)

        if when is None:
            make().start()
        else:
            pl.when(when)(lambda: make().start())
        sent.append((make, when))

    def arrive(ref, send_sem, recv_sem):
        remote(ref, ref, send_sem, recv_sem, {"tp": 1 - t}).wait_recv()

    planes = [nth_plane(f, nf, j) for j in range(nf)]

    def fpiece(slot, h):
        return fb.at[t, slot, pl.ds(h * (depth // 2), depth // 2)]

    def f_pass(slot):
        send(fb.at[t, slot], fb.at[t, slot], fp_s.at[slot], fp_r.at[slot], {"tp": 1 - t})

    def f_relay(p):
        slot = p * nr + r
        for h in range(2):
            for k, peer, piece in ((0, near, h), (1, side, 1 - h)):
                ref = fpiece(slot, piece)
                send(ref, ref, fn_s.at[k, p, piece], fn_r.at[k, p, piece], {"rep": peer})

    def f_far(p):
        one, two = p * nr + near, p * nr + side
        for k, slot, piece, to in ((0, one, 0, side), (1, two, 1, near)):
            ref = fpiece(slot, piece)
            arrive(ref, fn_s.at[k, p, piece], fn_r.at[k, p, piece])
            send(ref, ref, fd_s.at[p, piece], fd_r.at[p, piece], {"rep": to})
        for k, slot, piece in ((0, one, 1), (1, two, 0)):
            arrive(fpiece(slot, piece), fn_s.at[k, p, piece], fn_r.at[k, p, piece])
            f_pass(slot)

    def f_done(p):
        slot = p * nr + far
        for piece in range(2):
            arrive(fpiece(slot, piece), fd_s.at[p, piece], fd_r.at[p, piece])
        f_pass(slot)

    def f_tp(p):
        for row in ((near, side, far) if p is f else (r, near, side, far)):
            slot = p * nr + row
            ref = fb.at[1 - t, slot]
            arrive(ref, fp_s.at[slot], fp_r.at[slot])

    def wpiece(slot, p):
        if p == 0:
            return cwq.at[slot, :, pl.ds(0, cut)]
        if p == 2:
            return cwq.at[slot, :, pl.ds(cut, cols - cut)]
        at = pl.ds(0, cut) if p == 1 else pl.ds(cut, cols - cut)
        return cwo.at[slot, at] if aligned else cwo.at[slot, :, at]

    def w_xy(p, pieces):
        for piece in pieces:
            ref = wpiece(p * nr + r, piece)
            for k, peer in ((0, near), (1, side)):
                send(ref, ref, wn_s.at[k, p, piece], wn_r.at[k, p, piece], {"rep": peer})

    def w_far(p, pieces):
        one, two = p * nr + near, p * nr + side
        for piece in pieces:
            k, slot, to = ((0, one, side), (1, two, near))[piece % 2]
            ref = wpiece(slot, piece)
            arrive(ref, wn_s.at[k, p, piece], wn_r.at[k, p, piece])
            send(ref, ref, wd_s.at[p, piece], wd_r.at[p, piece], {"rep": to})

    def w_rest(p, pieces):
        one, two = p * nr + near, p * nr + side
        for piece in pieces:
            k, slot = ((1, two), (0, one))[piece % 2]
            ref = wpiece(slot, piece)
            arrive(ref, wn_s.at[k, p, piece], wn_r.at[k, p, piece])

    def w_last(p, pieces):
        for piece in pieces:
            ref = wpiece(p * nr + far, piece)
            arrive(ref, wd_s.at[p, piece], wd_r.at[p, piece])

    items = {0: ((0, 0), (1, 1), (2, 2), (3, 3)), 1: ((4, 0), (5, 1)), 2: ((6, 0), (7, 1)), 3: ((8, 0), (9, 1))}
    row_of = (r, near, side, far)

    def w_zown(*roles):
        for role in roles:
            for item, piece in items[role]:
                ref = wpiece(f * nr + row_of[role], piece)
                send(ref, ref, wz_s.at[f, item], wz_r.at[f, item], {"fs": f + 1}, f < nf - 1)
                send(ref, ref, wz_s.at[nf, item], wz_r.at[f, item], {"fs": f - 1}, f > 0)

    def w_zpass(j, *roles):
        p, sign = planes[j]
        to = f - sign
        for role in roles:
            for item, piece in items[role]:
                ref = wpiece(p * nr + row_of[role], piece)
                arrive(ref, wz_s.at[p, item], wz_r.at[p, item])
                inside = jnp.logical_and(to >= 0, to < nf)
                send(ref, ref, wz_s.at[p, item], wz_r.at[p, item], {"fs": to}, inside)

    def lowered(j):
        p = planes[j][0]
        for which in range(2):
            block = fb[which, pl.ds(p * nr, nr)].reshape(lane, rank)
            step = tokens // 2

            def one(i, carry):
                at = pl.ds(pl.multiple_of(i * step, 256), step)
                got = jnp.dot(
                    xs[which, at, pl.ds(pl.multiple_of(p * lane, 128), lane)], block, preferred_element_type=F32
                )
                if j > 0:
                    got = got + low[which, at]
                if j == nf - 1:
                    upper, lower = split_parts(got)
                    lows[0, at, which * rank : (which + 1) * rank] = upper
                    lows[1, at, which * rank : (which + 1) * rank] = lower
                else:
                    low[which, at] = got
                return carry

            lax.fori_loop(0, 2, one, 0)

    for df in range(1, nf):
        to = planes[df][0]
        ref = fb.at[t, me]
        send(ref, ref, fz_s.at[to], fz_r.at[f], {"fs": to})
    f_relay(f)
    for copy in weights:
        copy.wait()
    cwq[me] = encode(wq_ref[...])
    cwo[me] = encode(wo_ref[...]) if aligned else encode(wo_ref[...].T)
    w_xy(f, (0, 1))
    for j in range(1, nf):
        p = planes[j][0]
        slot = p * nr + r
        arrive(fb.at[t, slot], fz_s.at[p], fz_r.at[p])
        f_relay(p)
        f_pass(slot)
        if j == 1:
            w_zown(0)
        f_far(planes[j - 1][0])
        if j == 2:
            w_far(f, (0, 1))
            w_rest(f, (0, 1))
            w_zown(1, 2)
            for copy in big:
                copy.wait()
        if j == 3:
            w_last(f, (0, 1))
            w_zown(3)
        if j >= 2:
            f_done(planes[j - 2][0])
            f_tp(planes[j - 2][0])
            lowered(j - 2)
    f_far(planes[nf - 1][0])
    w_xy(f, (2, 3))
    f_done(planes[nf - 2][0])
    f_tp(planes[nf - 2][0])
    lowered(nf - 2)
    w_zpass(1, 0)
    f_done(planes[nf - 1][0])
    f_tp(planes[nf - 1][0])
    lowered(nf - 1)

    contract = (((0,), (0,)), ((), ()))
    for k, peer in ((2, far), (0, near), (1, side), (None, r)):
        at = pl.ds(pl.multiple_of(peer * quarter, 128), quarter)
        cot = cots[(peer * quarter) // rank]
        part = lax.dot_general(lows[0, :, at], cot, contract, preferred_element_type=F32) + lax.dot_general(
            lows[1, :, at], cot, contract, preferred_element_type=F32
        )
        part = part.reshape(nf, rows, cols)
        if k is None:
            own[...] = part
        else:
            outgoing[k] = part.astype(BF)
            send(outgoing.at[k], landed.at[k], a_s.at[k], a_r.at[k], {"rep": peer})
    w_far(f, (2, 3))
    w_xy(planes[1][0], (2, 3))
    w_zpass(1, 1, 2, 3)
    for k in range(3):
        arrive(landed.at[k], a_s.at[k], a_r.at[k])
    total = own[...] + landed[0].astype(F32) + landed[1].astype(F32) + landed[2].astype(F32)
    partial[...] = total.astype(BF)
    own[...] = total
    for j in range(1, nf):
        to = planes[j][0]
        send(partial.at[to], exchanged.at[f], b_s.at[to], b_r.at[f], {"fs": to})
    w_far(planes[1][0], (2, 3))
    mine = own[f]
    for j in range(1, nf):
        p = planes[j][0]
        arrive(exchanged.at[p], b_s.at[p], b_r.at[p])
        mine = mine + exchanged[p].astype(F32)
    whole[r, f] = mine.astype(BF)
    for j in range(nf):
        p = planes[j][0]
        ref = whole.at[r, p]
        if j == 0:
            for i in range(1, nf):
                to = planes[i][0]
                send(ref, ref, c_s.at[to], c_r.at[f], {"fs": to})
        else:
            arrive(ref, c_s.at[p], c_r.at[p])
        for k, peer in ((2, far), (0, near), (1, side)):
            send(ref, ref, e_s.at[k, p], e_r.at[k, p], {"rep": peer})
    w_zpass(2, 0)
    w_xy(planes[2][0], (2, 3))
    w_zpass(2, 1, 2, 3)
    for j in range(nf):
        p = planes[j][0]
        for k, peer in enumerate(peers):
            arrive(whole.at[peer, p], e_s.at[k, p], e_r.at[k, p])
    for copy in moments:
        copy.wait()
    half = nr // 2
    for which, first_ref, second_ref in ((0, nfq_ref, nsq_ref), (1, nfo_ref, nso_ref)):
        proj = whole[which * half : (which + 1) * half].astype(F32).reshape(rank, cols)
        if which:
            proj = proj.T
        moved = 0.9 * first_ref[...] + 0.1 * proj
        spread = 0.95 * second_ref[...] + 0.05 * proj * proj
        first_ref[...] = moved
        second_ref[...] = spread
        way = moved / (jnp.sqrt(spread) + 1e-08)
        upper, lower = split_parts(way)
        if which:
            flat[:, 0:rank] = upper
            flat[:, rank : 2 * rank] = lower
        else:
            dirs[0:rank] = upper
            dirs[rank : 2 * rank] = lower

    for j in range(3, nf):
        w_zpass(j, 0)
        w_xy(planes[j][0], (2, 3))
        w_far(planes[j - 1][0], (2, 3))

    def doubled(which, at, count):
        block = fb[which, pl.ds(at, count)].reshape(count * depth, rank)
        return jnp.concatenate([block, block], axis=1)

    across = (((1,), (1,)), ((), ()))

    def raw_q(at, count):
        return jnp.dot(doubled(0, at, count), dirs[...], preferred_element_type=F32)

    def raw_o(at, count):
        return lax.dot_general(flat[...], doubled(1, at, count), across, preferred_element_type=F32)

    def add(i, carry):
        one, two = carry
        raw = raw_q(i * nr, nr)
        one = one + jnp.sum((raw * raw).reshape(lane // 8, 8, cols), axis=0)
        raw = raw_o(i * nr, nr)
        two = two + jnp.sum((raw * raw).reshape(cols // 8, 8, lane), axis=0)
        return one, two

    one, two = lax.fori_loop(0, nf, add, (jnp.zeros((8, cols), F32), jnp.zeros((8, lane), F32)))
    square[0, 0] = jnp.full((8, 128), jnp.sum(one), F32)
    square[0, 1] = jnp.full((8, 128), jnp.sum(two), F32)
    copy = remote(square.at[0], square.at[1], x_s, x_r, {"tp": 1 - t})
    copy.start()
    for j in range(3, nf):
        w_zpass(j, 1, 2, 3)
    w_far(planes[nf - 1][0], (2, 3))
    copy.wait()
    entries = wide * cols * 2
    scale = [
        1.0 / jnp.sqrt((square[0, which, 0:1, 0:1] + square[1, which, 0:1, 0:1]) / entries + 0.01) for which in range(2)
    ]
    for raw, weight, new_weight, step_ref, which in (
        (raw_q(me, 1), wq_ref, nwq_ref, stq_ref, 0),
        (raw_o(me, 1), wo_ref, nwo_ref, sto_ref, 1),
    ):
        step = raw * scale[which]
        step_ref[...] = step
        new_weight[...] = weight[...] - 0.1 * step

    rate = [0.1 * scale[which] for which in range(2)]

    def finish(p):
        at = p * nr
        raw = raw_q(at, nr).reshape(nr, depth, cols)
        cq_ref[pl.ds(at, nr)] = (decode(cwq[pl.ds(at, nr)]) - rate[0] * raw).astype(BF)
        raw = raw_o(at, nr)
        if aligned:
            for k in range(nr):
                new = decode(cwo[at + k]) - rate[1] * raw[:, k * depth : (k + 1) * depth]
                co_ref[:, pl.ds(pl.multiple_of((at + k) * depth, 128), depth)] = new.astype(BF)
        else:
            new = decode(cwo[pl.ds(at, nr)]).reshape(lane, cols).T - rate[1] * raw
            co_ref[:, pl.ds(pl.multiple_of(p * lane, 128), lane)] = new.astype(BF)

    for j in range(nf):
        p = planes[j][0]
        w_rest(p, (2, 3))
        w_last(p, (2, 3))
        finish(p)
    for make, when in sent:
        if when is None:
            make().wait_send()
        else:
            pl.when(when)(lambda make=make: make().wait_send())


def store_kernel(count, *refs):
    ins, outs, sems = refs[:count], refs[count : 2 * count], refs[2 * count]
    copies = [pltpu.make_async_copy(ins[k], outs[k], sems.at[k]) for k in range(count)]
    for copy in copies:
        copy.start()
    for copy in copies:
        copy.wait()


def store(arrays):
    count = len(arrays)
    return pl.pallas_call(
        functools.partial(store_kernel, count),
        out_shape=[jax.ShapeDtypeStruct(a.shape, a.dtype) for a in arrays],
        in_specs=[pl.BlockSpec(memory_space=pltpu.VMEM)] * count,
        out_specs=[pl.BlockSpec(memory_space=pl.ANY)] * count,
        scratch_shapes=[pltpu.SemaphoreType.DMA((count,))],
        compiler_params=pltpu.CompilerParams(vmem_limit_bytes=16 * 1024 * 1024),
    )(*arrays)


def body(nf, nr, *args):
    saved_input, query_cotangent, saved_heads, block_cotangent, query_weight, output_weight = args[:6]
    query_factor, output_factor, query_first, query_second, output_first, output_second = args[6:]
    n = nf * nr
    depth, rank = query_factor.shape
    cols = query_weight.shape[1]
    tokens, width = saved_input.shape
    quarter = 2 * rank // nr
    rows = quarter // nf
    cut = cols // 4
    aligned = depth % 128 == 0
    dma = pltpu.SemaphoreType.DMA
    vmem = pl.BlockSpec(memory_space=pltpu.VMEM)
    shape = jax.ShapeDtypeStruct
    args = [pltpu.with_memory_space_constraint(a, pltpu.HBM) for a in args]
    outs = pl.pallas_call(
        functools.partial(update_kernel, nf, nr, n * depth, cut),
        out_shape=[
            shape((depth, cols), F32), shape((cols, depth), F32),
            shape((rank, cols), F32), shape((rank, cols), F32),
            shape((cols, rank), F32), shape((cols, rank), F32),
            shape((depth, cols), F32), shape((cols, depth), F32),
            shape((n, depth, cols), BF),
            shape((cols, n * depth), BF),
        ],
        in_specs=[pl.BlockSpec(memory_space=pltpu.HBM)] * 12,
        out_specs=[vmem] * 10,
        scratch_shapes=[
            pltpu.VMEM((2, tokens, width), BF),
            pltpu.VMEM((2, tokens, cols), BF),
            pltpu.VMEM((2, n, depth, rank), BF),
            pltpu.VMEM((depth, cols), F32), pltpu.VMEM((cols, depth), F32),
            pltpu.VMEM((n, depth, cols), BF), pltpu.VMEM((n, cols, depth) if aligned else (n, depth, cols), BF),
            pltpu.VMEM((2, tokens, rank), F32),
            pltpu.VMEM((2, tokens, 2 * rank), BF),
            pltpu.VMEM((3, nf, rows, cols), BF), pltpu.VMEM((3, nf, rows, cols), BF),
            pltpu.VMEM((nf, rows, cols), F32), pltpu.VMEM((nf, rows, cols), BF),
            pltpu.VMEM((nf, rows, cols), BF), pltpu.VMEM((nr, nf, rows, cols), BF),
            pltpu.VMEM((2 * rank, cols), BF), pltpu.VMEM((cols, 2 * rank), BF),
            pltpu.VMEM((2, 2, 8, 128), F32),
            dma((12,)),
            dma((nf,)), dma((nf,)), dma((2, nf, 2)), dma((2, nf, 2)), dma((nf, 2)), dma((nf, 2)), dma((n,)), dma((n,)),
            dma((2, nf, 4)), dma((2, nf, 4)), dma((nf, 4)), dma((nf, 4)), dma((nf + 1, 10)), dma((nf, 10)),
            dma((3,)), dma((3,)), dma((nf,)), dma((nf,)), dma((nf,)), dma((nf,)), dma((3, nf)), dma((3, nf)), dma, dma,
        ],
        compiler_params=pltpu.CompilerParams(
            collective_id=0, has_side_effects=True, vmem_limit_bytes=(44 if aligned else 52) * 1024 * 1024
        ),
    )(*[args[k] for k in (0, 3, 1, 2, 4, 5, 6, 7, 8, 9, 10, 11)])
    *rest, query_copy, output_copy = store(outs)
    return (*rest, query_copy.reshape(n * depth, cols), output_copy)


def solution(mesh):
    nf, nr = mesh.shape["fs"], mesh.shape["rep"]
    in_specs = (
        P(("fs", "rep"), None), P(("fs", "rep"), "tp"), P(("fs", "rep"), "tp"), P(("fs", "rep"), None),
        P(("fs", "rep"), "tp"), P("tp", ("fs", "rep")), P(("fs", "rep"), None), P(("fs", "rep"), None),
        P(None, "tp"), P(None, "tp"), P("tp", None), P("tp", None),
    )
    out_specs = (
        P(("fs", "rep"), "tp"), P("tp", ("fs", "rep")), P(None, "tp"), P(None, "tp"), P("tp", None), P("tp", None),
        P(("fs", "rep"), "tp"), P("tp", ("fs", "rep")), P(None, "tp"), P("tp", None),
    )
    return jax.shard_map(
        functools.partial(body, nf, nr), mesh=mesh, in_specs=in_specs, out_specs=out_specs, check_vma=False
    )
```

time: 109 us -> 79.1 us (0.73)
  Pallas kernels: 90.3 us -> 78.1 us
  matrix products: 11.1 us -> 0 us
  local copies, waits for them, and re-layouts: 3.36 us -> 0 us
  other arithmetic: 2.63 us -> 0 us
    pallas_call x2 -> x1, Pallas kernels: 87.1 us -> 75 us  [body(): pl.pallas_call(functools.partial(update_kernel, nf, nr, n * depth, cut),...]
    dot_general x6 -> x0, matrix products: 11.1 us -> none  [the longest x1 5.92 us: body(): cotan_low = jnp.dot(block_cotangent, whole_o, preferred_element_type=F32)]
    unnamed x24 -> x0, local copies, waits for them, and re-layouts: 3.15 us -> none
    convert_element_type x2 -> x0, other arithmetic: 2.56 us -> none  [encode(): return jnp.where(weight < 0, -size, size).astype(BF)]
where the time goes in v1:
time: 79.1 us; the launch traced here: 79 us
  Pallas kernels  78.1 us (99%)
  between operations  0.82 us (1%)
    pallas_call x1, Pallas kernels, body(): pl.pallas_call(functools.partial(update_kernel, nf, nr, n * depth, cut),...  75 us
    pallas_call x1, Pallas kernels, store(): pl.pallas_call(functools.partial(store_kernel, count), out_shape=[jax.Sha...  3.14 us

profile of v1, /device:TPU:0, one launch (start us, length us, event | category | flops | bytes accessed | tf_op | source)
XLA Modules:
  0.0 79.0 jit_solution(2542350263334830055)
XLA Ops:
  0.6 75.0 %shard_map.195 = (f32[128,512]{1,0:T(8,128)S(1)}, f32[512,128]{1,0:T(8,128)S(1)}, f32[256,512]{1,0:T(8,128)S(1)}, f32[256,512]{1,0:T(8,128)S(1)}, f32[512,256]{1...) custom-call(bf16[2048,2048]{1,0:T(8,128)(2,1)} %x_hbm.1, ...), custom_call_target="tpu_custom_call" | custom-call | tf_op jit(solution)/shard_map/pallas_call | solution.py:451
  75.7 3.1 %shard_map.196 = (f32[128,512]{1,0:T(8,128)}, f32[512,128]{1,0:T(8,128)}, f32[256,512]{1,0:T(8,128)}, f32[256,512]{1,0:T(8,128)}, f32[512,256]{1,0:T(8,128)}, /*...) custom-call(f32[128,512]{1,0:T(8,128)S(1)} %get-tuple-element.30.ref, ...), custom_call_target="tpu_custom_call" | custom-call | tf_op jit(solution)/shard_map/pallas_call | solution.py:426

commit v2 on v1

v2 whole, which is shorter than its diff:
```python
import functools

import jax
import jax.numpy as jnp
from jax import lax
from jax.experimental import pallas as pl
from jax.experimental.pallas import tpu as pltpu
from jax.sharding import PartitionSpec as P

MESH = pl.DeviceIdType.MESH
BF = jnp.bfloat16
F32 = jnp.float32

REACH = 6.0
SPAN = 120.0
PER_LOG = 1.0 / (2.0 * SPAN * 0.6931471805599453)


def split_parts(wide):
    upper = wide.astype(BF)
    lower = (wide - upper.astype(F32)).astype(BF)
    return (upper, lower)


def encode(weight):
    level = jnp.sqrt(jnp.minimum(jnp.abs(weight), REACH) * (1.0 / REACH))
    size = jnp.exp2(level * (2.0 * SPAN) - SPAN)
    return jnp.where(weight < 0, -size, size).astype(BF)


def decode(code):
    wide = code.astype(F32)
    level = jnp.log(jnp.abs(wide)) * PER_LOG + 0.5
    value = (REACH * level) * level
    return jnp.where(wide < 0, -value, value)


def remote(src, dst, send, recv, where):
    return pltpu.make_async_remote_copy(
        src_ref=src, dst_ref=dst, send_sem=send, recv_sem=recv, device_id=where, device_id_type=MESH
    )


def nth_plane(f, nf, j):
    if j == 0:
        return f, 0
    upper = (2 * f) // nf
    near_end = f + upper * (nf - 1 - 2 * f)
    over = jnp.minimum(1, j // (2 * near_end + 1))
    inner_sign = 1 if j % 2 else -1
    distance = over * (j - near_end) + (1 - over) * ((j + 1) // 2)
    sign = (1 - 2 * upper) * (over + (1 - over) * inner_sign)
    return f + sign * distance, distance


def update_kernel(
    nf, nr, wide,
    x_hbm, bc_hbm, qc_hbm, sh_hbm, wq_hbm, wo_hbm, fq_hbm, fo_hbm, mq_hbm, vq_hbm, mo_hbm, vo_hbm,
    nwq_out, nwo_out, nfq_out, nsq_out, nfo_out, nso_out, stq_out, sto_out, cq_out, co_out,
    nwq_ref, nwo_ref, nfq_ref, nsq_ref, nfo_ref, nso_ref, stq_ref, sto_ref, cq_ref, co_ref,
    xs, cots, fb, wq_ref, wo_ref, cwq, cwo, low, lows,
    mine, outgoing, landed, partial, exchanged, whole, dirs, flat, gram_q, gram_o, square,
    loc, put_s, fz_s, fz_r, fn_s, fn_r, fd_s, fd_r, fp_s, fp_r, wn_s, wn_r, wd_s, wd_r, wz_s, wz_r, wb_s, wb_r,
    a_s, a_r, b_s, b_r, c_s, c_r, e_s, e_r, g_s, g_r, h_s, h_r, x_s, x_r,
):
    f, r, t = lax.axis_index("fs"), lax.axis_index("rep"), lax.axis_index("tp")
    near = r + 1 - 2 * lax.rem(r, 2)
    side = lax.rem(r + 2, 4)
    far = 3 - r
    n = nf * nr
    me = f * nr + r
    depth, rank = fq_hbm.shape
    cols = wq_hbm.shape[1]
    tokens = x_hbm.shape[0]
    lane = nr * depth
    rows = rank // nf
    half = nr // 2
    span = cols // half
    peers = (near, side, far)
    aligned = depth % 128 == 0

    local = []

    def fetch(src, dst):
        copy = pltpu.make_async_copy(src, dst, loc.at[len(local)])
        copy.start()
        local.append(copy)
        return copy

    small = [fetch(fq_hbm, fb.at[0, me]), fetch(fo_hbm, fb.at[1, me])]
    weights = [fetch(wq_hbm, wq_ref), fetch(wo_hbm, wo_ref)]
    barrier = pltpu.get_barrier_semaphore()
    for df in range(1, nf):
        pl.semaphore_signal(barrier, inc=1, device_id={"fs": lax.rem(f + df, nf)}, device_id_type=MESH)
    for peer in peers:
        pl.semaphore_signal(barrier, inc=1, device_id={"rep": peer}, device_id_type=MESH)
    pl.semaphore_signal(barrier, inc=1, device_id={"tp": 1 - t}, device_id_type=MESH)
    first, second = t == 0, t == 1
    base = len(local)
    big = []
    for k, (when, src, dst) in enumerate((
        (first, x_hbm, xs), (second, bc_hbm, xs), (first, qc_hbm, cots.at[t]), (second, sh_hbm, cots.at[t]),
    )):
        def make(src=src, dst=dst, k=k):
            return pltpu.make_async_copy(src, dst, loc.at[base + k // 2])

        pl.when(when)(lambda make=make: make().start())
        big.append((when, make))
    local.extend(big[:2])
    moments = [fetch(a, b) for a, b in ((mq_hbm, nfq_ref), (vq_hbm, nsq_ref), (mo_hbm, nfo_ref), (vo_hbm, nso_ref))]
    for copy in small:
        copy.wait()
    pl.semaphore_wait(barrier, nf - 1 + 4)

    def put(src, dst, kind):
        pltpu.make_async_copy(src, dst, put_s.at[kind]).start()

    def gated(when, act):
        if when is None:
            act()
        else:
            pl.when(when)(act)

    def send(src, dst, send_sem, recv_sem, where, when=None):
        gated(when, lambda: remote(src, dst, send_sem, recv_sem, where).start())

    def arrive(ref, sem):
        remote(ref, ref, sem, sem, {"tp": 1 - t}).wait_recv()

    def settle(ref, sem, when=None):
        gated(when, lambda: remote(ref, ref, sem, sem, {"tp": 1 - t}).wait_send())

    def blocks(count):
        return cwq.at[pl.ds(0, count)]

    planes = [nth_plane(f, nf, j) for j in range(nf)]
    for when, src in ((first, sh_hbm), (second, qc_hbm)):
        send(src, cots.at[t], h_s, h_r, {"tp": 1 - t}, when)

    def fpiece(slot, h):
        return fb.at[t, slot, pl.ds(h * (depth // 2), depth // 2)]

    def f_pass(slot):
        send(fb.at[t, slot], fb.at[t, slot], fp_s, fp_r, {"tp": 1 - t})

    def f_relay(p):
        slot = p * nr + r
        for h in range(2):
            for k, peer, piece in ((0, near, h), (1, side, 1 - h)):
                ref = fpiece(slot, piece)
                send(ref, ref, fn_s, fn_r.at[k if piece == k else 2, p], {"rep": peer})

    def f_far(p):
        one, two = p * nr + near, p * nr + side
        for piece, slot, to in ((0, one, side), (1, two, near)):
            ref = fpiece(slot, piece)
            arrive(ref, fn_r.at[piece, p])
            send(ref, ref, fd_s, fd_r.at[p], {"rep": to})
        arrive(fb.at[t, one], fn_r.at[2, p])
        f_pass(one)
        f_pass(two)

    def f_done(p):
        slot = p * nr + far
        arrive(fb.at[t, slot], fd_r.at[p])
        f_pass(slot)

    def wpiece(slot, p):
        ref, count = ((cwq, depth), (cwo, cols if aligned else depth))[p % 2]
        return ref.at[slot, pl.ds(p // 2 * (count // 2), count // 2)]

    def chosen(j, pieces):
        for piece in pieces:
            if piece >= 2 or j == 0:
                yield piece, None
            elif j > 1:
                yield piece, planes[j][1] > 1

    def w_xy(j, pieces):
        p = planes[j][0]
        for piece, when in chosen(j, pieces):
            ref = wpiece(p * nr + r, piece)
            for k, peer in ((0, near), (1, side)):
                at = piece // 2 if piece % 2 == k else 2
                send(ref, ref, wn_s.at[p], wn_r.at[k, p, at], {"rep": peer}, when)

    def w_far(j, pieces):
        p = planes[j][0]
        one, two = p * nr + near, p * nr + side
        for piece, when in chosen(j, pieces):
            k = piece % 2
            ref = wpiece((one, two)[k], piece)
            gated(when, lambda: arrive(ref, wn_r.at[k, p, piece // 2]))
            send(ref, ref, wd_s.at[p], wd_r.at[p, piece // 2], {"rep": (side, near)[k]}, when)

    def w_rest(j):
        p, distance = planes[j]
        for k, ref in ((0, cwo.at[p * nr + near]), (1, cwq.at[p * nr + side])):
            part = wpiece(p * nr + (near, side)[k], 3 - k)
            if j != 1:
                gated(None if j == 0 else distance > 1, lambda: arrive(ref, wn_r.at[k, p, 2]))
            if j > 0:
                gated(distance == 1, lambda: arrive(part, wn_r.at[k, p, 2]))

    def w_last(j, half_of):
        p, distance = planes[j]
        if half_of or j != 1:
            when = None if half_of or j == 0 else distance > 1
            gated(when, lambda: arrive(cwq.at[p * nr + far], wd_r.at[p, half_of]))

    def w_out(j, when=None):
        to = planes[j][0]
        for piece in (2, 3, 0, 1):
            ref = wpiece(me, piece)
            send(ref, ref, wz_s, wz_r.at[f], {"fs": to}, when)

    def w_in(j):
        arrive(blocks(2), wz_r.at[planes[j][0]])

    def w_beside():
        for row in (near, side, far):
            for piece in (0, 1):
                ref = wpiece(f * nr + row, piece)
                send(ref, ref, wb_s.at[0], wb_r.at[f], {"fs": f + 1}, f < nf - 1)
                send(ref, ref, wb_s.at[1], wb_r.at[f], {"fs": f - 1}, f > 0)

    def lowered(j):
        p = planes[j][0]
        block = fb[t, pl.ds(p * nr, nr)].reshape(lane, rank)
        return jnp.dot(xs[:, pl.ds(pl.multiple_of(p * lane, 128), lane)], block, preferred_element_type=F32)

    for j in range(1, nf):
        to = planes[j][0]
        ref = fb.at[t, me]
        send(ref, ref, fz_s, fz_r.at[f], {"fs": to})
    f_relay(f)
    for copy in weights:
        copy.wait()
    cwq[me] = encode(wq_ref[...])
    cwo[me] = encode(wo_ref[...]) if aligned else encode(wo_ref[...].T)
    w_xy(0, (0,))
    for j in range(1, nf):
        p = planes[j][0]
        slot = p * nr + r
        arrive(fb.at[t, slot], fz_r.at[p])
        f_relay(p)
        f_pass(slot)
        if j == 1:
            w_xy(0, (1,))
        if j == nf - 1:
            for k in range(1, nf):
                w_out(k, planes[k][1] <= 2 if k > 2 else None)
        f_far(planes[j - 1][0])
    for j in range(nf - 2):
        f_done(planes[j][0])
    f_far(planes[nf - 1][0])
    w_xy(0, (2, 3))
    w_far(0, (0, 1))
    f_done(planes[nf - 2][0])
    for when, make in big:
        pl.when(when)(lambda make=make: make().wait())
    low[...] = sum(lowered(j) for j in range(nf - 1))
    f_done(planes[nf - 1][0])
    w_far(0, (2,))
    w_in(1)
    w_xy(1, (2, 3))
    lows[...] = (low[...] + lowered(nf - 1)).astype(BF)
    w_far(0, (3,))
    arrive(cots.at[1 - t], h_r)
    contract = (((0,), (0,)), ((), ()))
    for side_of, quarters in ((side // half, ((2, far), (1, side))), (r // half, ((0, near),))):
        part = lax.dot_general(lows[...], cots[side_of], contract, preferred_element_type=F32)
        for k in range(half):
            block = part[:, k * span : (k + 1) * span].reshape(nf, rows, span)
            mine[side_of * half + k] = block
            outgoing[side_of * half + k] = block.astype(BF)
        for k, peer in quarters:
            for j in range(nf - 1, -1, -1):
                p = planes[j][0]
                send(outgoing.at[peer, p], landed.at[k, p], a_s, a_r.at[p], {"rep": peer})
    w_last(0, 0)
    for j in range(nf - 1, -1, -1):
        p = planes[j][0]
        arrive(landed.at[:, p], a_r.at[p])
        total = mine[r, p] + landed[0, p].astype(F32) + landed[1, p].astype(F32) + landed[2, p].astype(F32)
        if j > 0:
            partial[p] = total.astype(BF)
            send(partial.at[p], exchanged.at[f], b_s, b_r.at[f], {"fs": p})
        else:
            result = total
    def hand(row):
        ref = whole.at[t, row]
        send(ref, ref, g_s, g_r, {"tp": 1 - t}, row // half == 1 - t)

    w_far(1, (2, 3))
    w_in(2)
    w_xy(2, (2, 3))
    for j in range(1, nf):
        p = planes[j][0]
        arrive(exchanged.at[p], b_r.at[p])
        result = result + exchanged[p].astype(F32)
    whole[t, r, f] = result.astype(BF)
    for j in range(nf):
        p = planes[j][0]
        ref = whole.at[t, r, p]
        if j == 0:
            for i in range(1, nf):
                to = planes[i][0]
                send(ref, ref, c_s, c_r.at[f], {"fs": to})
        else:
            arrive(ref, c_r.at[p])
        for k, peer in ((2, far), (0, near), (1, side)):
            send(ref, ref, e_s, e_r.at[k], {"rep": peer})
        if j == 0:
            for i in range(3, nf):
                w_out(i, planes[i][1] > 2)
    hand(r)
    w_far(2, (2, 3))
    w_xy(2, (0, 1))
    w_rest(0)
    w_beside()
    arrive(fb.at[1 - t, pl.ds(0, n - 1)], fp_r)
    for which in range(2):
        block = fb[which].reshape(wide, rank)
        upper, lower = split_parts(lax.dot_general(block, block, contract, preferred_element_type=F32))
        if which:
            gram_o[...] = jnp.concatenate([upper, lower, upper], axis=0)
        else:
            gram_q[...] = jnp.concatenate([upper, lower, upper], axis=1)
    for j in range(3, nf):
        w_in(j)
        w_xy(j, (2, 3))
    for k, peer in ((0, near), (1, side), (2, far)):
        arrive(whole.at[t, peer], e_r.at[k])
        hand(peer)
    arrive(whole.at[1 - t, pl.ds(t * half, half)], g_r)
    for copy in moments:
        copy.wait()
    norms = []
    for which, first_ref, second_ref in ((0, nfq_ref, nsq_ref), (1, nfo_ref, nso_ref)):
        proj = jnp.concatenate(
            [whole[which, t * half + k].astype(F32).reshape(rank, span) for k in range(half)], axis=1
        )
        if which:
            proj = proj.T
        moved = 0.9 * first_ref[...] + 0.1 * proj
        spread = 0.95 * second_ref[...] + 0.05 * proj * proj
        first_ref[...] = moved
        second_ref[...] = spread
        way = moved / (jnp.sqrt(spread) + 1e-08)
        upper, lower = split_parts(way)
        if which:
            flat[:, 0:rank] = upper
            flat[:, rank : 2 * rank] = lower
            shaped = jnp.dot(
                jnp.concatenate([upper, upper, lower], axis=1), gram_o[...], preferred_element_type=F32
            )
        else:
            dirs[0:rank] = upper
            dirs[rank : 2 * rank] = lower
            shaped = jnp.dot(
                gram_q[...], jnp.concatenate([upper, upper, lower], axis=0), preferred_element_type=F32
            )
        norms.append(jnp.sum(shaped * way))

    for src, dst in ((nfq_ref, nfq_out), (nsq_ref, nsq_out), (nfo_ref, nfo_out), (nso_ref, nso_out)):
        put(src, dst, 0)
    w_far(2, (0, 1))
    for j in range(3, nf):
        w_xy(j, (0, 1))

    def doubled(which, at, count):
        block = fb[which, pl.ds(at, count)].reshape(count * depth, rank)
        return jnp.concatenate([block, block], axis=1)

    across = (((1,), (1,)), ((), ()))

    def raw_q(at, count):
        return jnp.dot(doubled(0, at, count), dirs[...], preferred_element_type=F32)

    def raw_o(at, count):
        return lax.dot_general(flat[...], doubled(1, at, count), across, preferred_element_type=F32)

    square[0, 0] = jnp.full((8, 128), norms[0], F32)
    square[0, 1] = jnp.full((8, 128), norms[1], F32)
    copy = remote(square.at[0], square.at[1], x_s, x_r, {"tp": 1 - t})
    copy.start()
    for j in range(3, nf):
        w_far(j, (2, 3))
    copy.wait()
    entries = wide * cols * 2
    scale = [
        1.0 / jnp.sqrt(jnp.maximum(square[0, which, 0:1, 0:1] + square[1, which, 0:1, 0:1], 0.0) / entries + 0.01) for which in range(2)
    ]
    for raw, weight, new_weight, step_ref, which in (
        (raw_q(me, 1), wq_ref, nwq_ref, stq_ref, 0),
        (raw_o(me, 1), wo_ref, nwo_ref, sto_ref, 1),
    ):
        step = raw * scale[which]
        step_ref[...] = step
        new_weight[...] = weight[...] - 0.1 * step

    for src, dst in ((nwq_ref, nwq_out), (nwo_ref, nwo_out), (stq_ref, stq_out), (sto_ref, sto_out)):
        put(src, dst, 1)
    rate = [0.1 * scale[which] for which in range(2)]

    def finish(at, count):
        raw = raw_q(at, count).reshape(count, depth, cols)
        cq_ref[pl.ds(at, count)] = (decode(cwq[pl.ds(at, count)]) - rate[0] * raw).astype(BF)
        raw = raw_o(at, count)
        if aligned:
            for k in range(count):
                new = decode(cwo[at + k]) - rate[1] * raw[:, k * depth : (k + 1) * depth]
                co_ref[:, pl.ds(pl.multiple_of((at + k) * depth, 128), depth)] = new.astype(BF)
        else:
            new = decode(cwo[pl.ds(at, count)]).reshape(count * depth, cols).T - rate[1] * raw
            co_ref[:, pl.ds(pl.multiple_of(at * depth, 128), count * depth)] = new.astype(BF)
        block = pl.ds(at, count)
        put(cq_ref.at[block], cq_out.at[block], 2)
        block = pl.ds(pl.multiple_of(at * depth, 128), count * depth)
        put(co_ref.at[:, block], co_out.at[:, block], 3)

    for j in range(nf - 1):
        p = planes[j][0]
        if j > 0:
            w_rest(j)
            w_last(j, 0)
        w_last(j, 1)
        if j == 1:
            for step, when in ((1, f < nf - 1), (-1, f > 0)):
                gated(when, lambda: arrive(blocks(3), wb_r.at[f + step]))
        finish(p * nr, nr)
    for j in range(3, nf):
        w_far(j, (0, 1))
    p = planes[nf - 1][0]
    w_rest(nf - 1)
    if aligned:
        for row in (r, near, side):
            finish(p * nr + row, 1)
    w_last(nf - 1, 0)
    w_last(nf - 1, 1)
    if aligned:
        finish(p * nr + far, 1)
    else:
        finish(p * nr, nr)
    for kind, ref in ((0, cq_ref), (1, blocks(8)), (2, cq_ref), (3, co_ref)):
        pltpu.make_async_copy(ref, ref, put_s.at[kind]).wait()
    settle(fb.at[t, pl.ds(0, nf - 1)], fz_s)
    settle(fb.at[t, pl.ds(0, 2 * nf)], fn_s)
    settle(fb.at[t, pl.ds(0, nf)], fd_s)
    settle(fb.at[t, pl.ds(0, n - 1)], fp_s)
    for j in range(nf):
        p, distance = planes[j]
        if j != 1:
            full = None if j == 0 else distance > 1
            settle(blocks(4), wn_s.at[p], full)
            settle(blocks(2), wd_s.at[p], full)
        if j > 0:
            settle(blocks(2), wn_s.at[p], distance == 1)
            settle(blocks(1), wd_s.at[p], distance == 1)
    settle(blocks(2 * (nf - 1)), wz_s)
    settle(blocks(3), wb_s.at[0], f < nf - 1)
    settle(blocks(3), wb_s.at[1], f > 0)
    settle(outgoing.at[pl.ds(0, 3)], a_s)
    settle(partial.at[pl.ds(0, nf - 1)], b_s)
    settle(whole.at[t, r, pl.ds(0, nf - 1)], c_s)
    settle(whole.at[t, pl.ds(0, 3)], e_s)
    settle(whole.at[t, pl.ds(0, half)], g_s)
    settle(cots.at[t], h_s)


def store_kernel(count, *refs):
    ins, outs, sems = refs[:count], refs[count : 2 * count], refs[2 * count]
    copies = [pltpu.make_async_copy(ins[k], outs[k], sems.at[k]) for k in range(count)]
    for copy in copies:
        copy.start()
    for copy in copies:
        copy.wait()


def store(arrays):
    count = len(arrays)
    return pl.pallas_call(
        functools.partial(store_kernel, count),
        out_shape=[jax.ShapeDtypeStruct(a.shape, a.dtype) for a in arrays],
        in_specs=[pl.BlockSpec(memory_space=pl.ANY)] * count,
        out_specs=[pl.BlockSpec(memory_space=pl.ANY)] * count,
        scratch_shapes=[pltpu.SemaphoreType.DMA((count,))],
        compiler_params=pltpu.CompilerParams(vmem_limit_bytes=16 * 1024 * 1024),
    )(*arrays)


def body(nf, nr, *args):
    saved_input, query_cotangent, saved_heads, block_cotangent, query_weight, output_weight = args[:6]
    query_factor, output_factor, query_first, query_second, output_first, output_second = args[6:]
    n = nf * nr
    depth, rank = query_factor.shape
    cols = query_weight.shape[1]
    tokens, width = saved_input.shape
    rows = rank // nf
    span = 2 * cols // nr
    aligned = depth % 128 == 0
    dma = pltpu.SemaphoreType.DMA
    args = [pltpu.with_memory_space_constraint(a, pltpu.HBM) for a in args]
    results = [
        ((depth, cols), F32), ((cols, depth), F32),
        ((rank, cols), F32), ((rank, cols), F32), ((cols, rank), F32), ((cols, rank), F32),
        ((depth, cols), F32), ((cols, depth), F32),
        ((n, depth, cols), BF), ((cols, n * depth), BF),
    ]
    outs = pl.pallas_call(
        functools.partial(update_kernel, nf, nr, n * depth),
        out_shape=[jax.ShapeDtypeStruct(*one) for one in results],
        in_specs=[pl.BlockSpec(memory_space=pltpu.HBM)] * 12,
        out_specs=[pl.BlockSpec(memory_space=pl.ANY)] * 10,
        scratch_shapes=[pltpu.VMEM(*one) for one in results]
        + [
            pltpu.VMEM((tokens, width), BF),
            pltpu.VMEM((2, tokens, cols), BF),
            pltpu.VMEM((2, n, depth, rank), BF),
            pltpu.VMEM((depth, cols), F32), pltpu.VMEM((cols, depth), F32),
            pltpu.VMEM((n, depth, cols), BF), pltpu.VMEM((n, cols, depth) if aligned else (n, depth, cols), BF),
            pltpu.VMEM((tokens, rank), F32), pltpu.VMEM((tokens, rank), BF),
            pltpu.VMEM((nr, nf, rows, span), F32), pltpu.VMEM((nr, nf, rows, span), BF),
            pltpu.VMEM((3, nf, rows, span), BF), pltpu.VMEM((nf, rows, span), BF),
            pltpu.VMEM((nf, rows, span), BF), pltpu.VMEM((2, nr, nf, rows, span), BF),
            pltpu.VMEM((2 * rank, cols), BF), pltpu.VMEM((cols, 2 * rank), BF),
            pltpu.VMEM((rank, 3 * rank), BF), pltpu.VMEM((3 * rank, rank), BF),
            pltpu.VMEM((2, 2, 8, 128), F32),
            dma((10,)), dma((4,)),
            dma, dma((nf,)), dma, dma((3, nf)), dma, dma((nf,)), dma, dma,
            dma((nf,)), dma((2, nf, 3)), dma((nf,)), dma((nf, 2)), dma, dma((nf,)), dma((2,)), dma((nf,)),
            dma, dma((nf,)), dma, dma((nf,)), dma, dma((nf,)), dma, dma((3,)), dma, dma, dma, dma, dma, dma,
        ],
        compiler_params=pltpu.CompilerParams(
            collective_id=0, has_side_effects=True, vmem_limit_bytes=(41 if aligned else 49) * 1024 * 1024
        ),
    )(*[args[k] for k in (0, 3, 1, 2, 4, 5, 6, 7, 8, 9, 10, 11)])
    *rest, query_copy, output_copy = store(outs)
    return (*rest, query_copy.reshape(n * depth, cols), output_copy)


def solution(mesh):
    nf, nr = mesh.shape["fs"], mesh.shape["rep"]
    in_specs = (
        P(("fs", "rep"), None), P(("fs", "rep"), "tp"), P(("fs", "rep"), "tp"), P(("fs", "rep"), None),
        P(("fs", "rep"), "tp"), P("tp", ("fs", "rep")), P(("fs", "rep"), None), P(("fs", "rep"), None),
        P(None, "tp"), P(None, "tp"), P("tp", None), P("tp", None),
    )
    out_specs = (
        P(("fs", "rep"), "tp"), P("tp", ("fs", "rep")), P(None, "tp"), P(None, "tp"), P("tp", None), P("tp", None),
        P(("fs", "rep"), "tp"), P("tp", ("fs", "rep")), P(None, "tp"), P("tp", None),
    )
    return jax.shard_map(
        functools.partial(body, nf, nr), mesh=mesh, in_specs=in_specs, out_specs=out_specs, check_vma=False
    )
```

time: 79.1 us -> 69.9 us (0.88)
  Pallas kernels: 78.1 us -> 69 us
    pallas_call x1, Pallas kernels: 75 us -> 65.8 us  [body(): pl.pallas_call(functools.partial(update_kernel, nf, nr, n * depth), out_s...]
where the time goes in v2:
time: 69.9 us; the launch traced here: 69.8 us
  Pallas kernels  69 us (99%)
  between operations  0.82 us (1%)
    pallas_call x1, Pallas kernels, body(): pl.pallas_call(functools.partial(update_kernel, nf, nr, n * depth), out_s...  65.8 us
    pallas_call x1, Pallas kernels, store(): pl.pallas_call(functools.partial(store_kernel, count), out_shape=[jax.Sha...  3.14 us

profile of v2, /device:TPU:0, one launch (start us, length us, event | category | flops | bytes accessed | tf_op | source)
XLA Modules:
  0.0 69.8 jit_solution(6181041580983995779)
XLA Ops:
  0.6 65.8 %shard_map.195 = (f32[128,512]{1,0:T(8,128)S(1)}, f32[512,128]{1,0:T(8,128)S(1)}, f32[256,512]{1,0:T(8,128)S(1)}, f32[256,512]{1,0:T(8,128)S(1)}, f32[512,256]{1...) custom-call(bf16[2048,2048]{1,0:T(8,128)(2,1)} %x_hbm.1, ...), custom_call_target="tpu_custom_call" | custom-call | tf_op jit(solution)/shard_map/pallas_call | solution.py:511
  66.5 3.1 %shard_map.196 = (f32[128,512]{1,0:T(8,128)}, f32[512,128]{1,0:T(8,128)}, f32[256,512]{1,0:T(8,128)}, f32[256,512]{1,0:T(8,128)}, f32[512,256]{1,0:T(8,128)}, /*...) custom-call(f32[128,512]{1,0:T(8,128)S(1)} %get-tuple-element.30.ref, ...), custom_call_target="tpu_custom_call" | custom-call | tf_op jit(solution)/shard_map/pallas_call | solution.py:483

commit v3 on v2

--- a/solution.py
+++ b/solution.py
@@ -58,7 +58,7 @@
     x_hbm, bc_hbm, qc_hbm, sh_hbm, wq_hbm, wo_hbm, fq_hbm, fo_hbm, mq_hbm, vq_hbm, mo_hbm, vo_hbm,
     nwq_out, nwo_out, nfq_out, nsq_out, nfo_out, nso_out, stq_out, sto_out, cq_out, co_out,
     nwq_ref, nwo_ref, nfq_ref, nsq_ref, nfo_ref, nso_ref, stq_ref, sto_ref, cq_ref, co_ref,
-    xs, cots, fb, wq_ref, wo_ref, cwq, cwo, low, lows,
+    xs, cots, fb, wq_ref, wo_ref, cwq, cwo, low, lows, plain_q, plain_o, raws_q, raws_o,
     mine, outgoing, landed, partial, exchanged, whole, dirs, flat, gram_q, gram_o, square,
     loc, put_s, fz_s, fz_r, fn_s, fn_r, fd_s, fd_r, fp_s, fp_r, wn_s, wn_r, wd_s, wd_r, wz_s, wz_r, wb_s, wb_r,
     a_s, a_r, b_s, b_r, c_s, c_r, e_s, e_r, g_s, g_r, h_s, h_r, x_s, x_r,
@@ -227,7 +227,13 @@
     def lowered(j):
         p = planes[j][0]
         block = fb[t, pl.ds(p * nr, nr)].reshape(lane, rank)
-        return jnp.dot(xs[:, pl.ds(pl.multiple_of(p * lane, 128), lane)], block, preferred_element_type=F32)
+        got = jnp.dot(xs[:, pl.ds(pl.multiple_of(p * lane, 128), lane)], block, preferred_element_type=F32)
+        if j > 0:
+            got = got + low[...]
+        if j == nf - 1:
+            lows[...] = got.astype(BF)
+        else:
+            low[...] = got
 
     for j in range(1, nf):
         to = planes[j][0]
@@ -256,20 +262,16 @@
     f_far(planes[nf - 1][0])
     w_xy(0, (2, 3))
     w_far(0, (0, 1))
-    f_done(planes[nf - 2][0])
     for when, make in big:
         pl.when(when)(lambda make=make: make().wait())
-    low[...] = sum(lowered(j) for j in range(nf - 1))
-    f_done(planes[nf - 1][0])
-    w_far(0, (2,))
-    w_in(1)
-    w_xy(1, (2, 3))
-    lows[...] = (low[...] + lowered(nf - 1)).astype(BF)
-    w_far(0, (3,))
+    for j in range(nf):
+        p = planes[j][0]
+        if j >= nf - 2:
+            f_done(p)
+        lowered(j)
     arrive(cots.at[1 - t], h_r)
-    contract = (((0,), (0,)), ((), ()))
     for side_of, quarters in ((side // half, ((2, far), (1, side))), (r // half, ((0, near),))):
-        part = lax.dot_general(lows[...], cots[side_of], contract, preferred_element_type=F32)
+        part = lax.dot_general(lows[...], cots[side_of], (((0,), (0,)), ((), ())), preferred_element_type=F32)
         for k in range(half):
             block = part[:, k * span : (k + 1) * span].reshape(nf, rows, span)
             mine[side_of * half + k] = block
@@ -279,6 +281,7 @@
                 p = planes[j][0]
                 send(outgoing.at[peer, p], landed.at[k, p], a_s, a_r.at[p], {"rep": peer})
     w_last(0, 0)
+    w_far(0, (2, 3))
     for j in range(nf - 1, -1, -1):
         p = planes[j][0]
         arrive(landed.at[:, p], a_r.at[p])
@@ -292,9 +295,17 @@
         ref = whole.at[t, row]
         send(ref, ref, g_s, g_r, {"tp": 1 - t}, row // half == 1 - t)
 
-    w_far(1, (2, 3))
-    w_in(2)
-    w_xy(2, (2, 3))
+    def weights_o(at, count):
+        if aligned:
+            return jnp.concatenate([decode(cwo[at + k]) for k in range(count)], axis=1)
+        return decode(cwo[pl.ds(at, count)]).reshape(count * depth, cols).T
+
+    def plain(p, at, count):
+        plain_q[...] = decode(cwq[pl.ds(at, count)])
+        plain_o[...] = weights_o(at, count)
+
+    w_in(1)
+    w_xy(1, (2, 3))
     for j in range(1, nf):
         p = planes[j][0]
         arrive(exchanged.at[p], b_r.at[p])
@@ -314,22 +325,27 @@
         if j == 0:
             for i in range(3, nf):
                 w_out(i, planes[i][1] > 2)
+            w_far(1, (2, 3))
+            w_in(2)
+            w_xy(2, (2, 3))
     hand(r)
-    w_far(2, (2, 3))
     w_xy(2, (0, 1))
     w_rest(0)
     w_beside()
     arrive(fb.at[1 - t, pl.ds(0, n - 1)], fp_r)
     for which in range(2):
         block = fb[which].reshape(wide, rank)
-        upper, lower = split_parts(lax.dot_general(block, block, contract, preferred_element_type=F32))
+        upper, lower = split_parts(lax.dot_general(block, block, (((0,), (0,)), ((), ())), preferred_element_type=F32))
         if which:
             gram_o[...] = jnp.concatenate([upper, lower, upper], axis=0)
         else:
             gram_q[...] = jnp.concatenate([upper, lower, upper], axis=1)
+    w_last(0, 1)
+    plain(f, f * nr, nr)
+    w_far(2, (2, 3))
     for j in range(3, nf):
         w_in(j)
-        w_xy(j, (2, 3))
+        w_xy(j, (2, 3, 0, 1))
     for k, peer in ((0, near), (1, side), (2, far)):
         arrive(whole.at[t, peer], e_r.at[k])
         hand(peer)
@@ -366,8 +382,6 @@
     for src, dst in ((nfq_ref, nfq_out), (nsq_ref, nsq_out), (nfo_ref, nfo_out), (nso_ref, nso_out)):
         put(src, dst, 0)
     w_far(2, (0, 1))
-    for j in range(3, nf):
-        w_xy(j, (0, 1))
 
     def doubled(which, at, count):
         block = fb[which, pl.ds(at, count)].reshape(count * depth, rank)
@@ -385,6 +399,10 @@
     square[0, 1] = jnp.full((8, 128), norms[1], F32)
     copy = remote(square.at[0], square.at[1], x_s, x_r, {"tp": 1 - t})
     copy.start()
+    for j in range(2):
+        p = planes[j][0]
+        raws_q[j] = raw_q(p * nr, nr).reshape(nr, depth, cols)
+        raws_o[j] = raw_o(p * nr, nr)
     for j in range(3, nf):
         w_far(j, (2, 3))
     copy.wait()
@@ -404,17 +422,14 @@
         put(src, dst, 1)
     rate = [0.1 * scale[which] for which in range(2)]
 
-    def finish(at, count):
-        raw = raw_q(at, count).reshape(count, depth, cols)
-        cq_ref[pl.ds(at, count)] = (decode(cwq[pl.ds(at, count)]) - rate[0] * raw).astype(BF)
-        raw = raw_o(at, count)
-        if aligned:
-            for k in range(count):
-                new = decode(cwo[at + k]) - rate[1] * raw[:, k * depth : (k + 1) * depth]
-                co_ref[:, pl.ds(pl.multiple_of((at + k) * depth, 128), depth)] = new.astype(BF)
-        else:
-            new = decode(cwo[pl.ds(at, count)]).reshape(count * depth, cols).T - rate[1] * raw
-            co_ref[:, pl.ds(pl.multiple_of(at * depth, 128), count * depth)] = new.astype(BF)
+    def finish(at, count, j=nf):
+        old = plain_q[...] if j == 0 else decode(cwq[pl.ds(at, count)])
+        raw = raws_q[j] if j < 2 else raw_q(at, count).reshape(count, depth, cols)
+        cq_ref[pl.ds(at, count)] = (old - rate[0] * raw).astype(BF)
+        old = plain_o[...] if j == 0 else weights_o(at, count)
+        raw = raws_o[j] if j < 2 else raw_o(at, count)
+        across_at = pl.ds(pl.multiple_of(at * depth, 128), count * depth)
+        co_ref[:, across_at] = (old - rate[1] * raw).astype(BF)
         block = pl.ds(at, count)
         put(cq_ref.at[block], cq_out.at[block], 2)
         block = pl.ds(pl.multiple_of(at * depth, 128), count * depth)
@@ -425,22 +440,22 @@
         if j > 0:
             w_rest(j)
             w_last(j, 0)
-        w_last(j, 1)
+            w_last(j, 1)
         if j == 1:
             for step, when in ((1, f < nf - 1), (-1, f > 0)):
                 gated(when, lambda: arrive(blocks(3), wb_r.at[f + step]))
-        finish(p * nr, nr)
-    for j in range(3, nf):
-        w_far(j, (0, 1))
+        if j == nf - 2:
+            for i in range(3, nf):
+                w_far(i, (0, 1))
+        finish(p * nr, nr, j)
     p = planes[nf - 1][0]
     w_rest(nf - 1)
     if aligned:
-        for row in (r, near, side):
-            finish(p * nr + row, 1)
+        finish(p * nr + r // 2 * 2, 2)
     w_last(nf - 1, 0)
     w_last(nf - 1, 1)
     if aligned:
-        finish(p * nr + far, 1)
+        finish(p * nr + far // 2 * 2, 2)
     else:
         finish(p * nr, nr)
     for kind, ref in ((0, cq_ref), (1, blocks(8)), (2, cq_ref), (3, co_ref)):
@@ -521,6 +536,8 @@
             pltpu.VMEM((depth, cols), F32), pltpu.VMEM((cols, depth), F32),
             pltpu.VMEM((n, depth, cols), BF), pltpu.VMEM((n, cols, depth) if aligned else (n, depth, cols), BF),
             pltpu.VMEM((tokens, rank), F32), pltpu.VMEM((tokens, rank), BF),
+            pltpu.VMEM((nr, depth, cols), F32), pltpu.VMEM((cols, nr * depth), F32),
+            pltpu.VMEM((2, nr, depth, cols), F32), pltpu.VMEM((2, cols, nr * depth), F32),
             pltpu.VMEM((nr, nf, rows, span), F32), pltpu.VMEM((nr, nf, rows, span), BF),
             pltpu.VMEM((3, nf, rows, span), BF), pltpu.VMEM((nf, rows, span), BF),
             pltpu.VMEM((nf, rows, span), BF), pltpu.VMEM((2, nr, nf, rows, span), BF),
@@ -533,7 +550,7 @@
             dma, dma((nf,)), dma, dma((nf,)), dma, dma((nf,)), dma, dma((3,)), dma, dma, dma, dma, dma, dma,
         ],
         compiler_params=pltpu.CompilerParams(
-            collective_id=0, has_side_effects=True, vmem_limit_bytes=(41 if aligned else 49) * 1024 * 1024
+            collective_id=0, has_side_effects=True, vmem_limit_bytes=(46 if aligned else 54) * 1024 * 1024
         ),
     )(*[args[k] for k in (0, 3, 1, 2, 4, 5, 6, 7, 8, 9, 10, 11)])
     *rest, query_copy, output_copy = store(outs)

time: 69.9 us -> 65.5 us (0.937)
  Pallas kernels: 69 us -> 64.5 us
    pallas_call x1, Pallas kernels: 65.8 us -> 61.4 us  [body(): pl.pallas_call(functools.partial(update_kernel, nf, nr, n * depth), out_s...]
where the time goes in v3:
time: 65.5 us; the launch traced here: 65.3 us
  Pallas kernels  64.5 us (98%)
  between operations  0.82 us (1%)
    pallas_call x1, Pallas kernels, body(): pl.pallas_call(functools.partial(update_kernel, nf, nr, n * depth), out_s...  61.4 us
    pallas_call x1, Pallas kernels, store(): pl.pallas_call(functools.partial(store_kernel, count), out_shape=[jax.Sha...  3.14 us

profile of v3, /device:TPU:0, one launch (start us, length us, event | category | flops | bytes accessed | tf_op | source)
XLA Modules:
  0.0 65.3 jit_solution(14537479544066295455)
XLA Ops:
  0.6 61.4 %shard_map.195 = (f32[128,512]{1,0:T(8,128)S(1)}, f32[512,128]{1,0:T(8,128)S(1)}, f32[256,512]{1,0:T(8,128)S(1)}, f32[256,512]{1,0:T(8,128)S(1)}, f32[512,256]{1...) custom-call(bf16[2048,2048]{1,0:T(8,128)(2,1)} %x_hbm.1, ...), custom_call_target="tpu_custom_call" | custom-call | tf_op jit(solution)/shard_map/pallas_call | solution.py:526
  62.0 3.1 %shard_map.196 = (f32[128,512]{1,0:T(8,128)}, f32[512,128]{1,0:T(8,128)}, f32[256,512]{1,0:T(8,128)}, f32[256,512]{1,0:T(8,128)}, f32[512,256]{1,0:T(8,128)}, /*...) custom-call(f32[128,512]{1,0:T(8,128)S(1)} %get-tuple-element.30.ref, ...), custom_call_target="tpu_custom_call" | custom-call | tf_op jit(solution)/shard_map/pallas_call | solution.py:498

commit v4 on v3

--- a/solution.py
+++ b/solution.py
@@ -256,15 +256,18 @@
         if j == nf - 1:
             for k in range(1, nf):
                 w_out(k, planes[k][1] <= 2 if k > 2 else None)
+        if j == nf - 1:
+            f_done(f)
+            for when, make in big:
+                pl.when(when)(lambda make=make: make().wait())
+            lowered(0)
         f_far(planes[j - 1][0])
-    for j in range(nf - 2):
+    for j in range(1, nf - 2):
         f_done(planes[j][0])
     f_far(planes[nf - 1][0])
     w_xy(0, (2, 3))
     w_far(0, (0, 1))
-    for when, make in big:
-        pl.when(when)(lambda make=make: make().wait())
-    for j in range(nf):
+    for j in range(1, nf):
         p = planes[j][0]
         if j >= nf - 2:
             f_done(p)
@@ -331,7 +334,6 @@
     hand(r)
     w_xy(2, (0, 1))
     w_rest(0)
-    w_beside()
     arrive(fb.at[1 - t, pl.ds(0, n - 1)], fp_r)
     for which in range(2):
         block = fb[which].reshape(wide, rank)
@@ -342,6 +344,7 @@
             gram_q[...] = jnp.concatenate([upper, lower, upper], axis=1)
     w_last(0, 1)
     plain(f, f * nr, nr)
+    w_beside()
     w_far(2, (2, 3))
     for j in range(3, nf):
         w_in(j)
@@ -399,12 +402,14 @@
     square[0, 1] = jnp.full((8, 128), norms[1], F32)
     copy = remote(square.at[0], square.at[1], x_s, x_r, {"tp": 1 - t})
     copy.start()
+    for j in range(3, nf):
+        w_far(j, (2, 3))
     for j in range(2):
         p = planes[j][0]
         raws_q[j] = raw_q(p * nr, nr).reshape(nr, depth, cols)
         raws_o[j] = raw_o(p * nr, nr)
     for j in range(3, nf):
-        w_far(j, (2, 3))
+        w_far(j, (0, 1))
     copy.wait()
     entries = wide * cols * 2
     scale = [
@@ -444,9 +449,6 @@
         if j == 1:
             for step, when in ((1, f < nf - 1), (-1, f > 0)):
                 gated(when, lambda: arrive(blocks(3), wb_r.at[f + step]))
-        if j == nf - 2:
-            for i in range(3, nf):
-                w_far(i, (0, 1))
         finish(p * nr, nr, j)
     p = planes[nf - 1][0]
     w_rest(nf - 1)

time: 65.5 us -> 65.6 us (level)
  no operation moved by 1% of the time
where the time goes in v4:
time: 65.6 us; the launch traced here: 65.5 us
  Pallas kernels  64.7 us (99%)
  between operations  0.82 us (1%)
    pallas_call x1, Pallas kernels, body(): pl.pallas_call(functools.partial(update_kernel, nf, nr, n * depth), out_s...  61.5 us
    pallas_call x1, Pallas kernels, store(): pl.pallas_call(functools.partial(store_kernel, count), out_shape=[jax.Sha...  3.14 us

profile of v4, /device:TPU:0, one launch (start us, length us, event | category | flops | bytes accessed | tf_op | source)
XLA Modules:
  0.0 65.5 jit_solution(9165589645925275051)
XLA Ops:
  0.6 61.5 %shard_map.195 = (f32[128,512]{1,0:T(8,128)S(1)}, f32[512,128]{1,0:T(8,128)S(1)}, f32[256,512]{1,0:T(8,128)S(1)}, f32[256,512]{1,0:T(8,128)S(1)}, f32[512,256]{1...) custom-call(bf16[2048,2048]{1,0:T(8,128)(2,1)} %x_hbm.1, ...), custom_call_target="tpu_custom_call" | custom-call | tf_op jit(solution)/shard_map/pallas_call | solution.py:528
  62.2 3.1 %shard_map.196 = (f32[128,512]{1,0:T(8,128)}, f32[512,128]{1,0:T(8,128)}, f32[256,512]{1,0:T(8,128)}, f32[256,512]{1,0:T(8,128)}, f32[512,256]{1,0:T(8,128)}, /*...) custom-call(f32[128,512]{1,0:T(8,128)S(1)} %get-tuple-element.30.ref, ...), custom_call_target="tpu_custom_call" | custom-call | tf_op jit(solution)/shard_map/pallas_call | solution.py:500
